TPU v7x, 512 devices: a whole 4x8x8 slice. The times are simulated.
512 devices in a mesh: sp: 64 (over z, y), tp: 8 (over x, core).
Axes of the slice: x: 4, y: 8, z: 8, core: 2. Of those that a mesh axis runs over, the one named last changes fastest.
Arguments:
- tokens: bfloat16 [12288, 4096], P('sp'), may hold values from -6 to 6
- norm_gain: float32 [4096], replicated, may hold values from 0.1 to 1.9
- conv_value: bfloat16 [4096, 2048], P('sp', 'tp'), may hold values from -0.09375 to 0.09375
- conv_gate: bfloat16 [4096, 2048], P('sp', 'tp'), may hold values from -0.09375 to 0.09375
- state_feed: bfloat16 [4096, 2048], P('sp', 'tp'), may hold values from -0.09375 to 0.09375
- conv_taps: float32 [31, 2048], P(None, 'tp'), may hold values from -1 to 1
- chan_gain: float32 [2048], replicated, may hold values from 0.1 to 1.9
- chan_shift: float32 [2048], replicated, may hold values from -3 to 3
- conv_project: bfloat16 [2048, 4096], P('sp', 'tp'), may hold values from -0.125 to 0.125
- decay_rate: float32 [128, 64], P('tp'), may hold values from 0.1 to 3
- frequency: float32 [128, 64], P('tp'), may hold values from 0.1 to 3
- input_real: float32 [128, 64, 16], P('tp'), may hold values from -0.01953125 to 0.01953125
- input_imag: float32 [128, 64, 16], P('tp'), may hold values from -0.01953125 to 0.01953125
- output_real: float32 [128, 16, 64], P('tp'), may hold values from -0.5 to 0.5
- output_imag: float32 [128, 16, 64], P('tp'), may hold values from -0.5 to 0.5
- skip_gain: float32 [2048], P('tp'), may hold values from -3 to 3
- state_value: bfloat16 [2048, 4096], P('sp', 'tp'), may hold values from -0.125 to 0.125
- state_gate: bfloat16 [2048, 4096], P('sp', 'tp'), may hold values from -0.125 to 0.125
- initial_state: float32 [2, 128, 64], P(None, 'tp'), may hold values from -5 to 5
Outputs:
- mixer_out: bfloat16 [12288, 4096], P('sp', 'tp')
- final_state: float32 [2, 128, 64], P(None, 'tp')
All inputs are finite; a program needn't handle non-finite values.
Results may differ from a plain program's by a relative error of at most 0.0085.
Values may be sent and summed in bfloat16 or wider, within the bound.
A program may use at most 64 MiB of HBM per device.

v0:
```python
import jax
import jax.numpy as jnp
from jax import lax
from jax.sharding import PartitionSpec as P


def passed_along(value, axis, steps):
    count = lax.axis_size(axis)
    leading, last = (max(0, -steps), min(count, count - steps))
    return lax.ppermute(value, axis, [(source, source + steps) for source in range(leading, last)])


def laid_out(pieces, dim):
    pieces = jnp.moveaxis(pieces, 0, dim)
    dims = pieces.shape
    return pieces.reshape(*dims[:dim], dims[dim] * dims[dim + 1], *dims[dim + 2 :])


def copy_for_each(shard, axis):
    length = lax.axis_size(axis)
    return lax.all_to_all(
        jnp.broadcast_to(shard[None], (length, *shard.shape)), axis, 0, 0, tiled=True
    )


def gathered_copies(shard, axis, dim):
    return laid_out(copy_for_each(shard, axis), dim)


def sent_together(arrays, axis, dim, along):
    ends, at = ([], 0)
    for a in arrays[:-1]:
        at += a.shape[along]
        ends.append(at)
    both = jnp.concatenate(arrays, axis=along)
    return tuple(jnp.split(gathered_copies(both, axis, dim), ends, axis=along))


def rotate(first_real, first_imag, second_real, second_imag):
    return (
        first_real * second_real - first_imag * second_imag,
        first_real * second_imag + first_imag * second_real,
    )


def power_table(base_real, base_imag, exponent, largest):
    result_real = jnp.ones((exponent.shape[0], base_real.shape[0]), jnp.float32)
    result_imag = jnp.zeros((exponent.shape[0], base_real.shape[0]), jnp.float32)
    square_real, square_imag = (base_real, base_imag)
    for place in range(max(largest, 1).bit_length()):
        chosen = (exponent >> place & 1 == 1)[:, None]
        next_real, next_imag = rotate(result_real, result_imag, square_real, square_imag)
        result_real = jnp.where(chosen, next_real, result_real)
        result_imag = jnp.where(chosen, next_imag, result_imag)
        square_real, square_imag = rotate(square_real, square_imag, square_real, square_imag)
    return (result_real, result_imag)


def local(
    tokens,
    norm_gain,
    conv_value,
    conv_gate,
    state_feed,
    conv_taps,
    chan_gain,
    chan_shift,
    conv_project,
    decay_rate,
    frequency,
    input_real,
    input_imag,
    output_real,
    output_imag,
    skip_gain,
    state_value,
    state_gate,
    initial_state,
):
    floats = tokens.astype(jnp.float32)
    normed = (
        floats * lax.rsqrt(jnp.mean(floats * floats, axis=1, keepdims=True) + 1e-06) * norm_gain
    ).astype(jnp.bfloat16)
    length = tokens.shape[0]
    width = conv_value.shape[1]
    in_block = jnp.concatenate([conv_value, conv_gate, state_feed], axis=1)
    projected = jnp.dot(
        normed,
        lax.all_gather(in_block, "sp", axis=0, tiled=True),
        preferred_element_type=jnp.float32,
    )
    gated_linear = (projected[:, :width] * jax.nn.sigmoid(projected[:, width : 2 * width])).astype(
        jnp.bfloat16
    )
    state_drive = projected[:, 2 * width :].astype(jnp.bfloat16)
    kernel = conv_taps.shape[0]
    before = passed_along(gated_linear[length - (kernel - 1) :], "sp", 1)
    padded = jnp.concatenate([before, gated_linear], axis=0).astype(jnp.float32)
    conv_sum = jnp.zeros((length, width), jnp.float32)
    for offset in range(kernel):
        conv_sum = conv_sum + conv_taps[offset] * padded[offset : offset + length]
    conv_out = conv_sum.astype(jnp.bfloat16)
    seq_devices = lax.axis_size("sp")
    total_tokens = length * seq_devices
    groups, state_size, group_size = input_real.shape
    flat = groups * state_size
    rate_real = -decay_rate / total_tokens
    magnitude = jnp.exp(rate_real)
    step_real = magnitude * jnp.cos(frequency)
    step_imag = magnitude * jnp.sin(frequency)
    modulus = rate_real * rate_real + frequency * frequency
    lift_real = step_real - 1.0
    factor_real = (lift_real * rate_real + step_imag * frequency) / modulus
    factor_imag = (step_imag * rate_real - lift_real * frequency) / modulus
    drive_real = factor_real[..., None] * input_real - factor_imag[..., None] * input_imag
    drive_imag = factor_real[..., None] * input_imag + factor_imag[..., None] * input_real
    grouped = state_drive.astype(jnp.float32).reshape(length, groups, group_size)
    pushed_real = jnp.einsum("gph,tgh->tgp", drive_real, grouped).reshape(length, flat)
    pushed_imag = jnp.einsum("gph,tgh->tgp", drive_imag, grouped).reshape(length, flat)
    base_real = step_real.reshape(flat)
    base_imag = step_imag.reshape(flat)
    square_size = base_real * base_real + base_imag * base_imag
    back_real = base_real / square_size
    back_imag = -base_imag / square_size
    positions = lax.iota(jnp.int32, length)
    counted = positions + 1
    power_real, power_imag = power_table(base_real, base_imag, counted, length)
    undo_real, undo_imag = power_table(back_real, back_imag, counted, length)
    scaled_real, scaled_imag = rotate(undo_real, undo_imag, pushed_real, pushed_imag)
    lower = (positions[:, None] >= positions[None, :]).astype(jnp.float32)
    summed_real = jnp.dot(lower, scaled_real)
    summed_imag = jnp.dot(lower, scaled_imag)
    local_real, local_imag = rotate(power_real, power_imag, summed_real, summed_imag)
    span_real, span_imag = (power_real[-1], power_imag[-1])
    last_real, last_imag = (local_real[-1], local_imag[-1])
    start_real = initial_state[0].reshape(flat)
    start_imag = initial_state[1].reshape(flat)
    finals = gathered_copies(jnp.stack([last_real, last_imag])[None], "sp", 0)
    position = lax.axis_index("sp")
    device_ids = lax.iota(jnp.int32, seq_devices)
    lag = jnp.maximum(position - 1 - device_ids, 0)
    weight_real, weight_imag = power_table(span_real, span_imag, lag, seq_devices)
    before_mask = (device_ids < position).astype(jnp.float32)[:, None]
    moved_real, moved_imag = rotate(weight_real, weight_imag, finals[:, 0], finals[:, 1])
    lead_real, lead_imag = power_table(
        span_real, span_imag, jnp.stack([position, jnp.int32(seq_devices)]), seq_devices
    )
    opening_real, opening_imag = rotate(lead_real[0], lead_imag[0], start_real, start_imag)
    entry_real = opening_real + jnp.sum(moved_real * before_mask, axis=0)
    entry_imag = opening_imag + jnp.sum(moved_imag * before_mask, axis=0)
    tail_real, tail_imag = power_table(
        span_real, span_imag, seq_devices - 1 - device_ids, seq_devices
    )
    carried_real, carried_imag = rotate(tail_real, tail_imag, finals[:, 0], finals[:, 1])
    closing_real, closing_imag = rotate(lead_real[1], lead_imag[1], start_real, start_imag)
    final_real = closing_real + jnp.sum(carried_real, axis=0)
    final_imag = closing_imag + jnp.sum(carried_imag, axis=0)
    final_state = jnp.stack([final_real, final_imag]).reshape(2, groups, state_size)
    state_real = (power_real * entry_real - power_imag * entry_imag + local_real).reshape(
        length, groups, state_size
    )
    state_imag = (power_real * entry_imag + power_imag * entry_real + local_imag).reshape(
        length, groups, state_size
    )
    response = jnp.einsum("ghp,tgp->tgh", output_real, state_real) - jnp.einsum(
        "ghp,tgp->tgh", output_imag, state_imag
    )
    response = response.reshape(length, groups * group_size) + skip_gain * state_drive.astype(
        jnp.float32
    )
    activated = jax.nn.gelu(response).astype(jnp.bfloat16)
    conv_rows, activated_rows = sent_together((conv_out, activated), "tp", 1, 0)
    conv_full = conv_rows.astype(jnp.float32)
    row_mean = jnp.mean(conv_full, axis=1, keepdims=True)
    centred = conv_full - row_mean
    variance = jnp.mean(centred * centred, axis=1, keepdims=True)
    conv_act = jax.nn.silu(centred * lax.rsqrt(variance + 1e-05) * chan_gain + chan_shift).astype(
        jnp.bfloat16
    )
    columns = conv_project.shape[1]
    out_block = jnp.concatenate([conv_project, state_value, state_gate], axis=1)
    piece = lax.all_gather(out_block, "sp", axis=0, tiled=True)
    conv_branch = jnp.dot(conv_act, piece[:, :columns], preferred_element_type=jnp.float32)
    state_both = jnp.dot(activated_rows, piece[:, columns:], preferred_element_type=jnp.float32)
    mixer_out = (
        conv_branch + state_both[:, :columns] * jax.nn.sigmoid(state_both[:, columns:])
    ).astype(jnp.bfloat16)
    return (mixer_out, final_state)


def solution(mesh):
    in_specs = (
        P("sp", None),
        P(),
        P("sp", "tp"),
        P("sp", "tp"),
        P("sp", "tp"),
        P(None, "tp"),
        P(),
        P(),
        P("sp", "tp"),
        P("tp", None),
        P("tp", None),
        P("tp", None, None),
        P("tp", None, None),
        P("tp", None, None),
        P("tp", None, None),
        P("tp"),
        P("sp", "tp"),
        P("sp", "tp"),
        P(None, "tp", None),
    )
    out_specs = (P("sp", "tp"), P(None, "tp", None))
    return jax.shard_map(local, mesh=mesh, in_specs=in_specs, out_specs=out_specs, check_vma=False)
```

profile of v0, /device:TPU:1, one launch (start us, length us, event | category | flops | bytes accessed | tf_op | source)
XLA Modules:
  0.0 217.5 jit_solution(8492768212598717211)
XLA Ops:
  7.2 1.6 pad_maximum_fusion.1
  8.9 1.4 pad_maximum_fusion.2
  12.8 3.0 %add_select_fusion.5 = f32[192,1024]{1,0:T(8,128)S(1)} fusion(f32[1024]{0:T(1024)S(1)} %get-tuple-element.130, f32[1024]{0:T(1024)S(1)} %get-tuple-element.129, pred[192]{0:T(512)(128)(4,1)S(1)} %get-tuple-element.142, f32[1024]{0:T(1024)S(1)} %get-tuple-element.132, f32[1024]{0:T(1024)S(1)} %get-tuple-element.131, f32[1024]{0:T(1024)S(1)} %get-tuple-element.133, ...), kind=kLoop, calls=%fused_computation.81 | loop fusion | flops 10616832 | bytes 853504 | tf_op jit(solution)/shard_map/jit(_where)/select_n | solution.py:54
  15.8 3.0 %subtract_select_fusion.5 = f32[192,1024]{1,0:T(8,128)S(1)} fusion(f32[1024]{0:T(1024)S(1)} %get-tuple-element.130, f32[1024]{0:T(1024)S(1)} %get-tuple-element.129, pred[192]{0:T(512)(128)(4,1)S(1)} %get-tuple-element.142, f32[1024]{0:T(1024)S(1)} %get-tuple-element.132, f32[1024]{0:T(1024)S(1)} %get-tuple-element.131, f32[1024]{0:T(1024)S(1)} %get-tuple-element.133, ...), kind=kLoop, calls=%fused_computation.82 | loop fusion | flops 10616832 | bytes 853504 | tf_op jit(solution)/shard_map/jit(_where)/select_n | solution.py:53
  27.9 78.0 %all-gather.3.cloned.1.call-done = bf16[4096,768]{1,0:T(8,128)(2,1)} async-done(((bf16[64,768]{1,0:T(8,128)(2,1)}), bf16[4096,768]{1,0:T(8,128)(2,1)}) %all-gather.3.cloned.1.call-update) | async-done | bytes 6291472 | tf_op jit(solution)/shard_map/all_gather | solution.py:89
  105.9 4.2 %fusion.9 = f32[192,768]{1,0:T(8,128)S(1)} fusion(bf16[4096,768]{1,0:T(8,128)(2,1)} %all-gather.3.cloned.1.call-done, bf16[192,4096]{1,0:T(8,128)(2,1)S(1)} %copy-done.1, f32[4096]{0:T(1024)S(1)} %copy-done.140, f32[192]{0:T(256)S(1)} %add_rsqrt_fusion.1), kind=kOutput, calls=%fused_computation.14 | convolution fusion | flops 1211105280 | bytes 8471296 | tf_op jit(solution)/shard_map/dot_general | solution.py:87
  113.8 2.7 %fusion.48 = f32[192,1024]{1,0:T(8,128)S(1)} fusion(f32[192,1024]{1,0:T(8,128)S(1)} %copy.40, f32[192,1024]{1,0:T(8,128)S(1)} %copy.39, f32[1024]{0:T(1024)} %get-tuple-element.115, f32[1024]{0:T(1024)} %get-tuple-element.114, pred[192]{0:T(512)(128)(4,1)S(1)} %copy-done.99, f32[1024]{0:T(1024)} %get-tuple-element.117, f32[1024]{0:T(1024)} %get-tuple-element.116, ...), kind=kOutput, calls=%fused_computation.67 | convolution fusion | flops 87527424 | bytes 2426368 | tf_op jit(solution)/shard_map/dot_general | solution.py:131
  116.8 4.6 %multiply_subtract_fusion = (f32[192,1024]{1,0:T(8,128)S(1)}, f32[192,1024]{1,0:T(8,128)S(1)}) fusion(f32[192,1024]{1,0:T(8,128)S(1)} %fusion.48, f32[1024]{0:T(1024)S(1)} %copy-done.33, f32[1024]{0:T(1024)S(1)} %copy-done.31, f32[1024]{0:T(1024)S(1)} %copy-done.37, f32[1024]{0:T(1024)S(1)} %copy-done.35, f32[1024]{0:T(1024)S(1)} %copy-done.39, ...), kind=kOutput, calls=%fused_computation.62 | convolution fusion | flops 99520512 | bytes 4064768 | tf_op jit(solution)/shard_map/dot_general | solution.py:132
  121.4 6.8 %multiply_add_fusion = f32[192,1024]{1,0:T(8,128)S(1)} fusion(f32[192,1024]{1,0:T(8,128)S(1)} %fusion.48, f32[192,1024]{1,0:T(8,128)S(1)} %get-tuple-element.126, f32[1024]{0:T(1024)S(1)} %copy-done.33, f32[1024]{0:T(1024)S(1)} %copy-done.31, f32[1024]{0:T(1024)S(1)} %copy-done.37, f32[1024]{0:T(1024)S(1)} %copy-done.35, f32[1024]{0:T(1024)S(1)} %copy-done.39, ...), kind=kLoop, calls=%fused_computation.61 | loop fusion | flops 11993088 | bytes 2426368 | tf_op jit(solution)/shard_map/add | solution.py:42
  129.4 9.2 %all-to-all-start = ((f32[64,1,2,1024]{3,2,1,0:T(2,128)}), f32[64,1,2,1024]{3,2,1,0:T(2,128)S(1)}, u32[]{:S(2)}, u32[]{:S(2)}) async-start(f32[64,1,2,1024]{3,2,1,0:T(2,128)} %broadcast_in_dim.579), calls=%async_computation | async-start | bytes 1048576 | tf_op jit(solution)/shard_map/all_to_all | solution.py:21
  139.7 3.1 %collective-permute-start = (bf16[30,256]{1,0:T(8,128)(2,1)S(1)}, bf16[30,256]{1,0:T(8,128)(2,1)S(1)}, u32[]{:S(2)}, u32[]{:S(2)}) collective-permute-start(bf16[30,256]{1,0:T(8,128)(2,1)S(1)} %slice.335), channel_id=1, source_target_pairs={{0,8},{8,16},{16,24},{24,32},{32,40},{40,48},{48,56},{56,64},{64,7... | collective-permute-start | bytes 46088 | tf_op jit(solution)/shard_map/ppermute | solution.py:10
  143.0 4.1 %collective-permute-done = bf16[30,256]{1,0:T(8,128)(2,1)S(1)} collective-permute-done((bf16[30,256]{1,0:T(8,128)(2,1)S(1)}, bf16[30,256]{1,0:T(8,128)(2,1)S(1)}, u32[]{:S(2)}, u32[]{:S(2)}) %collective-permute-start) | collective-permute-done | bytes 15392 | tf_op jit(solution)/shard_map/ppermute | solution.py:10
  148.1 8.0 %all-to-all-done = f32[64,1,2,1024]{3,2,1,0:T(2,128)S(1)} async-done(((f32[64,1,2,1024]{3,2,1,0:T(2,128)}), f32[64,1,2,1024]{3,2,1,0:T(2,128)S(1)}, u32[]{:S(2)}, u32[]{:S(2)}) %all-to-all-start) | async-done | bytes 524320 | tf_op jit(solution)/shard_map/all_to_all | solution.py:21
  156.7 1.7 fusion.85
  158.4 1.1 fusion.83
  160.9 4.5 %add_add_fusion = bf16[192,1024]{1,0:T(8,128)(2,1)S(1)} fusion(f32[192,1024]{1,0:T(8,128)S(1)} %multiply_add_fusion, f32[1024]{0:T(1024)S(1)} %bitcast.192, f32[1024]{0:T(1024)S(1)} %bitcast.194, f32[1024]{0:T(1024)S(1)} %copy-done.33, f32[1024]{0:T(1024)S(1)} %copy-done.31, f32[1024]{0:T(1024)S(1)} %copy-done.37, f32[1024]{0:T(1024)S(1)} %copy-done.35, ...), kind=kLoop, calls=%fused_computation.59 | loop fusion | flops 12386304 | bytes 1254912 | tf_op jit(solution)/shard_map/add | solution.py:162
  165.6 4.5 %subtract_add_fusion = bf16[192,1024]{1,0:T(8,128)(2,1)S(1)} fusion(f32[192,1024]{1,0:T(8,128)S(1)} %get-tuple-element.125, f32[1024]{0:T(1024)S(1)} %bitcast.193, f32[1024]{0:T(1024)S(1)} %bitcast.195, f32[1024]{0:T(1024)S(1)} %copy-done.33, f32[1024]{0:T(1024)S(1)} %copy-done.31, f32[1024]{0:T(1024)S(1)} %copy-done.37, f32[1024]{0:T(1024)S(1)} %copy-done.35, ...), kind=kLoop, calls=%fused_computation.60 | loop fusion | flops 12386304 | bytes 1254912 | tf_op jit(solution)/shard_map/add | solution.py:159
  170.9 1.3 broadcast_in_dim.580
  172.2 7.6 %all-to-all-start.1 = ((bf16[8,384,256]{2,1,0:T(8,128)(2,1)}), bf16[8,384,256]{2,1,0:T(8,128)(2,1)S(1)}, u32[]{:S(2)}, u32[]{:S(2)}) async-start(bf16[8,384,256]{2,1,0:T(8,128)(2,1)} %broadcast_in_dim.580), calls=%async_computation.1 | async-start | bytes 3145728 | tf_op jit(solution)/shard_map/all_to_all | solution.py:21
  180.5 19.8 %all-to-all-done.1 = bf16[8,384,256]{2,1,0:T(8,128)(2,1)S(1)} async-done(((bf16[8,384,256]{2,1,0:T(8,128)(2,1)}), bf16[8,384,256]{2,1,0:T(8,128)(2,1)S(1)}, u32[]{:S(2)}, u32[]{:S(2)}) %all-to-all-start.1) | async-done | bytes 1572896 | tf_op jit(solution)/shard_map/all_to_all | solution.py:21
  200.6 1.1 copy.52
  202.4 1.8 all-gather.5.cloned.1.call-done
  204.2 3.4 %fusion = f32[192,1024]{1,0:T(8,128)S(1)} fusion(bf16[192,2048]{1,0:T(8,128)(2,1)} %bitcast.127, bf16[2048,1536]{1,0:T(8,128)(2,1)} %all-gather.5.cloned.1.call-done), kind=kOutput, calls=%fused_computation | convolution fusion | flops 805306368 | bytes 5767168 | tf_op jit(solution)/shard_map/dot_general | solution.py:184
  207.6 3.0 %fusion.16 = bf16[192,512]{1,0:T(8,128)(2,1)} fusion(bf16[2048,1536]{1,0:T(8,128)(2,1)} %all-gather.5.cloned.1.call-done, f32[192,2048]{1,0:T(8,128)S(1)} %bitcast.123, f32[2048]{0:T(1024)S(1)} %copy-done.141, f32[2048]{0:T(1024)S(1)} %copy-done.142, f32[192]{0:T(256)S(1)} %add_rsqrt_fusion, f32[192]{0:T(256)S(1)} %broadcast_multiply_fusion, ...), kind=kOutput, calls=%fused_computation.31 | convolution fusion | flops 406781952 | bytes 4670976 | tf_op jit(solution)/shard_map/dot_general | solution.py:183
  (360 shorter events, 21.5 us)
Async XLA Ops:
  7.2 163.1 %copy-start = (f32[16,16,64]{2,1,0:T(8,128)S(1)}, f32[16,16,64]{2,1,0:T(8,128)}, u32[]{:S(2)}) copy-start(f32[16,16,64]{2,1,0:T(8,128)} %param.32) | copy-start | bytes 196612
  7.2 98.7 %all-gather.3.cloned.1.call-start = ((), (), s32[]{:S(2)}) async-start(), calls=%async_computation.2 | async-start | bytes 6389760 | tf_op jit(solution)/shard_map/all_gather | solution.py:89
  8.8 195.4 %all-gather.5.cloned.1.call-start = ((), (), s32[]{:S(2)}) async-start(), calls=%async_computation.3 | async-start | bytes 6389760 | tf_op jit(solution)/shard_map/all_gather | solution.py:182
  11.2 100.0 %copy-start.61 = (f32[16,64]{1,0:T(8,128)}, f32[16,64]{1,0:T(8,128)S(1)}, u32[]{:S(2)}) copy-start(f32[16,64]{1,0:T(8,128)S(1)} %get-tuple-element.85) | copy-start | bytes 12292
  11.2 100.0 %copy-start.63 = (f32[16,64]{1,0:T(8,128)}, f32[16,64]{1,0:T(8,128)S(1)}, u32[]{:S(2)}) copy-start(f32[16,64]{1,0:T(8,128)S(1)} %get-tuple-element.86) | copy-start | bytes 12292
  15.8 90.1 %copy-start.140 = (f32[4096]{0:T(1024)S(1)}, f32[4096]{0:T(1024)}, u32[]{:S(2)}) copy-start(f32[4096]{0:T(1024)} %param.20) | copy-start | bytes 49156
  22.5 87.6 %copy-start.10 = (f32[1,1024]{1,0:T(1,128)}, f32[1,1024]{1,0:T(1,128)S(1)}, u32[]{:S(2)}) copy-start(f32[1,1024]{1,0:T(1,128)S(1)} %get-tuple-element.13) | copy-start | bytes 12292
  22.5 87.6 %copy-start.12 = (f32[1,1024]{1,0:T(1,128)}, f32[1,1024]{1,0:T(1,128)S(1)}, u32[]{:S(2)}) copy-start(f32[1,1024]{1,0:T(1,128)S(1)} %get-tuple-element.14) | copy-start | bytes 12292
  22.5 87.6 %copy-start.14 = (f32[1,1024]{1,0:T(1,128)}, f32[1,1024]{1,0:T(1,128)S(1)}, u32[]{:S(2)}) copy-start(f32[1,1024]{1,0:T(1,128)S(1)} %get-tuple-element.12) | copy-start | bytes 12292
  22.5 87.6 %copy-start.44 = (f32[1,1024]{1,0:T(1,128)}, f32[1,1024]{1,0:T(1,128)S(1)}, u32[]{:S(2)}) copy-start(f32[1,1024]{1,0:T(1,128)S(1)} %get-tuple-element.17) | copy-start | bytes 12292
  22.6 87.6 %copy-start.46 = (f32[1,1024]{1,0:T(1,128)}, f32[1,1024]{1,0:T(1,128)S(1)}, u32[]{:S(2)}) copy-start(f32[1,1024]{1,0:T(1,128)S(1)} %get-tuple-element.18) | copy-start | bytes 12292
  22.6 87.6 %copy-start.52 = (f32[1,1024]{1,0:T(1,128)}, f32[1,1024]{1,0:T(1,128)S(1)}, u32[]{:S(2)}) copy-start(f32[1,1024]{1,0:T(1,128)S(1)} %get-tuple-element.19) | copy-start | bytes 12292
  22.6 87.6 %copy-start.54 = (f32[1,1024]{1,0:T(1,128)}, f32[1,1024]{1,0:T(1,128)S(1)}, u32[]{:S(2)}) copy-start(f32[1,1024]{1,0:T(1,128)S(1)} %get-tuple-element.20) | copy-start | bytes 12292
  22.6 87.6 %copy-start.56 = (f32[1,1024]{1,0:T(1,128)}, f32[1,1024]{1,0:T(1,128)S(1)}, u32[]{:S(2)}) copy-start(f32[1,1024]{1,0:T(1,128)S(1)} %get-tuple-element.21) | copy-start | bytes 12292
  22.6 87.6 %copy-start.58 = (f32[1,1024]{1,0:T(1,128)}, f32[1,1024]{1,0:T(1,128)S(1)}, u32[]{:S(2)}) copy-start(f32[1,1024]{1,0:T(1,128)S(1)} %get-tuple-element.22) | copy-start | bytes 12292
  23.8 86.4 %copy-start.8 = (f32[1,1024]{1,0:T(1,128)}, f32[1,1024]{1,0:T(1,128)S(1)}, u32[]{:S(2)}) copy-start(f32[1,1024]{1,0:T(1,128)S(1)} %add_multiply_fusion.7) | copy-start | bytes 12292
  23.8 86.4 %copy-start.48 = (f32[1024]{0:T(1024)}, f32[1024]{0:T(1024)S(1)}, u32[]{:S(2)}) copy-start(f32[1024]{0:T(1024)S(1)} %get-tuple-element.99) | copy-start | bytes 12292
  23.8 86.4 %copy-start.50 = (f32[1024]{0:T(1024)}, f32[1024]{0:T(1024)S(1)}, u32[]{:S(2)}) copy-start(f32[1024]{0:T(1024)S(1)} %get-tuple-element.100) | copy-start | bytes 12292
  27.9 83.4 %copy-start.4 = (f32[16,64,16]{1,2,0:T(8,128)S(1)}, f32[16,64,16]{1,2,0:T(8,128)}, u32[]{:S(2)}) copy-start(f32[16,64,16]{1,2,0:T(8,128)} %param.30) | copy-start | bytes 196612
  27.9 83.4 %copy-start.6 = (f32[16,64,16]{1,2,0:T(8,128)S(1)}, f32[16,64,16]{1,2,0:T(8,128)}, u32[]{:S(2)}) copy-start(f32[16,64,16]{1,2,0:T(8,128)} %param.31) | copy-start | bytes 196612
  128.2 19.0 %copy-start.108 = (f32[1,256]{1,0:T(1,128)S(1)}, f32[1,256]{1,0:T(1,128)}, u32[]{:S(2)}) copy-start(f32[1,256]{1,0:T(1,128)} %get-tuple-element.46) | copy-start | bytes 3076
  129.4 26.7 %all-to-all-start = ((f32[64,1,2,1024]{3,2,1,0:T(2,128)}), f32[64,1,2,1024]{3,2,1,0:T(2,128)S(1)}, u32[]{:S(2)}, u32[]{:S(2)}) async-start(f32[64,1,2,1024]{3,2,1,0:T(2,128)} %broadcast_in_dim.579), calls=%async_computation | async-start | bytes 1048576 | tf_op jit(solution)/shard_map/all_to_all | solution.py:21
  139.7 7.4 %collective-permute-start = (bf16[30,256]{1,0:T(8,128)(2,1)S(1)}, bf16[30,256]{1,0:T(8,128)(2,1)S(1)}, u32[]{:S(2)}, u32[]{:S(2)}) collective-permute-start(bf16[30,256]{1,0:T(8,128)(2,1)S(1)} %slice.335), channel_id=1, source_target_pairs={{0,8},{8,16},{16,24},{24,32},{32,40},{40,48},{48,56},{56,64},{64,7... | collective-permute-start | bytes 46088 | tf_op jit(solution)/shard_map/ppermute | solution.py:10
  172.2 28.1 %all-to-all-start.1 = ((bf16[8,384,256]{2,1,0:T(8,128)(2,1)}), bf16[8,384,256]{2,1,0:T(8,128)(2,1)S(1)}, u32[]{:S(2)}, u32[]{:S(2)}) async-start(bf16[8,384,256]{2,1,0:T(8,128)(2,1)} %broadcast_in_dim.580), calls=%async_computation.1 | async-start | bytes 3145728 | tf_op jit(solution)/shard_map/all_to_all | solution.py:21
  (124 other events, 1004.1 us)
Sparse Core Ops, SparseCore 0:
  11.0 94.8 all-gather.2
  109.4 94.6 all-gather.4
where the time goes:
time: 218 us; the launch traced here: 217 us
  waiting for transfers between devices  112 us (51%)
  other arithmetic  40.3 us (18%)
  starting transfers between devices  20 us (9%)
  matrix products  19 us (9%)
  between operations  16.4 us (8%)
  local copies, waits for them, and re-layouts  9.94 us (5%)
    all_gather x1, waiting for transfers between devices, local(): lax.all_gather(in_block, 'sp', axis=0, tiled=True)  78 us
    all_to_all x2, waiting for transfers between devices, copy_for_each(): lax.all_to_all(jnp.broadcast_to(shard[None], (length, *shard.shape)), axi...  27.8 us
    all_to_all x2, starting transfers between devices, copy_for_each(): lax.all_to_all(jnp.broadcast_to(shard[None], (length, *shard.shape)), axi...  16.8 us
    add x3, other arithmetic, rotate(): first_real * second_imag + first_imag * second_real  7.44 us
    dot_general x1, matrix products, local(): summed_imag = jnp.dot(lower, scaled_imag)  4.6 us
    add x1, other arithmetic, local(): power_real * entry_real - power_imag * entry_imag + local_real  4.47 us
    add x1, other arithmetic, local(): power_real * entry_imag + power_imag * entry_real + local_imag  4.46 us
  transfers between devices with their start and end apart: 5, of which 5 were waited for; matrix products, arithmetic and copies ran while one was open for 27% of the time, Pallas kernels for 0%

commit v1 on v0

v1 whole, which is shorter than its diff:
```python
import jax
import jax.numpy as jnp
from jax import lax
from jax.experimental import pallas as pl
from jax.experimental.pallas import tpu as pltpu
from jax.sharding import PartitionSpec as P

BF, F32 = jnp.bfloat16, jnp.float32
HIGHEST = lax.Precision.HIGHEST
MESH = pl.DeviceIdType.MESH
SIDE = 8
CHIPS = 4
NT = (((1,), (1,)), ((), ()))


def hops(direction, half):
    return SIDE // 2 if (direction > 0) == (half == 0) else SIDE // 2 - 1


SLOTS = [
    (direction, half, k)
    for direction in (1, -1)
    for half in (0, 1)
    for k in range(hops(direction, half))
]
SLOT_OF = {slot: at for at, slot in enumerate(SLOTS)}


def rotate(first_real, first_imag, second_real, second_imag):
    return (
        first_real * second_real - first_imag * second_imag,
        first_real * second_imag + first_imag * second_real,
    )


def iota(shape, dim):
    return lax.broadcasted_iota(jnp.int32, shape, dim)


def kernel(
    tokens, norm_gain, conv_value, conv_gate, state_feed, conv_taps, chan_gain, chan_shift,
    conv_project, decay_rate, frequency, input_real, input_imag, output_real, output_imag,
    skip_gain, state_value, state_gate, initial_state,
    out, final_state,
    ws1, wc1, ws2, wc2, raw, normed, result,
    power_r, power_i, undo_r, undo_i, drive_r, drive_i, emit, feed, scaled, summed, states,
    rows, finals, totals, gated, halo, padded, shifted, conv_all, act_all, conv_act, mixed,
    load_sem, ring_send, ring_recv, scan_send, scan_recv, halo_sem, tp_send, tp_recv,
):
    seq = lax.axis_index("sp")
    t = lax.axis_index("tp")
    z, y = seq // SIDE, seq % SIDE
    chip, core = t // 2, t % 2
    length = tokens.shape[0]
    groups, size, wide = input_real.shape
    flat = groups * size
    width = groups * wide

    def device(zz, yy, tt):
        return {"sp": zz * SIDE + yy, "tp": tt}

    def step_to(at, by, count):
        return lax.rem(at + by + count, count)

    def remote(src, dst, send, recv, to):
        return pltpu.make_async_remote_copy(
            src_ref=src, dst_ref=dst, send_sem=send, recv_sem=recv, device_id=to, device_id_type=MESH
        )

    events = []
    sent = []

    def at(time, fn):
        events.append((time, len(events), fn))

    loads = {}

    def load(name, index, src, dst):
        loads[name] = pltpu.make_async_copy(src, dst, load_sem.at[index])
        loads[name].start()

    load("ws1", 0, state_feed, ws1.at[z, y])
    load("wc1v", 1, conv_value, wc1.at[0, z, y])
    load("wc1g", 2, conv_gate, wc1.at[1, z, y])
    load("ws2v", 3, state_value, ws2.at[0, z, y])
    load("ws2g", 4, state_gate, ws2.at[1, z, y])
    load("wc2", 5, conv_project, wc2.at[z, y])
    load("raw", 6, tokens, raw)

    barrier = pltpu.get_barrier_semaphore()
    here = {"z": z, "y": y}
    following = lax.rem(seq + 1, SIDE * SIDE)
    preceding = lax.rem(seq + SIDE * SIDE - 1, SIDE * SIDE)
    partners = []
    for d in range(1, SIDE):
        partners.append(device(z, step_to(y, d, SIDE), t))
        partners.append(device(step_to(z, d, SIDE), y, t))
    for d in range(1, 2 * CHIPS):
        partners.append(device(z, y, step_to(t, d, 2 * CHIPS)))
    partners.append({"sp": following, "tp": t})
    partners.append({"sp": preceding, "tp": t})
    for partner in partners:
        pl.semaphore_signal(barrier, inc=1, device_id=partner, device_id_type=MESH)
    pl.semaphore_wait(barrier, len(partners))

    def ring(number, axis, block, start, tau, ready):
        position = here[axis]

        def neighbour(direction):
            beside = step_to(position, direction, SIDE)
            return device(beside, y, t) if axis == "z" else device(z, beside, t)

        def copy(direction, half, k, source):
            slot = SLOT_OF[(direction, half, k)]
            return remote(
                block(source, half), block(source, half),
                ring_send.at[number, slot], ring_recv.at[number, slot], neighbour(direction),
            )

        def send(direction, half, k):
            moving = copy(direction, half, k, step_to(position, -direction * k, SIDE))
            moving.start()
            sent.append(moving)

        def first():
            ready()
            for half in (0, 1):
                for direction in (1, -1):
                    send(direction, half, 0)

        at(start, first)

        def arrived(direction, half, k):
            source = step_to(position, -direction * (k + 1), SIDE)
            copy(direction, half, k, source).wait_recv()
            if k + 1 < hops(direction, half):
                send(direction, half, k + 1)

        last = start
        for k in range(SIDE // 2):
            for half in (0, 1):
                for direction in (1, -1):
                    if k < hops(direction, half):
                        time = start + tau * k + (half + 1) * tau / 2 + 1.7
                        last = max(last, time)
                        at(time, lambda a=direction, b=half, c=k: arrived(a, b, c))
        return last

    def nothing():
        pass

    def loaded(*names):
        def wait():
            for name in names:
                loads[name].wait()
        return wait

    quarter = SIDE // 2
    deep1, deep2 = ws1.shape[2] // 2, wc2.shape[2] // 2

    def rows_of(half, deep):
        return pl.ds(half * deep, deep)

    ring(0, "y", lambda i, h: ws1.at[z, i, rows_of(h, deep1)], 0.0, 0.8, loaded("ws1"))
    ring(1, "z", lambda i, h: wc1.at[h, i, y], 0.1, 1.4, loaded("wc1v", "wc1g"))
    s1 = ring(2, "z", lambda i, h: ws1.at[i, pl.ds(h * quarter, quarter)], 9.0, 5.6, nothing)
    c1 = ring(3, "y", lambda i, h: wc1.at[:, pl.ds(h * quarter, quarter), i], 12.5, 11.2, nothing)
    p2 = ring(4, "y", lambda i, h: ws2.at[h, z, i], 15.0, 3.0, loaded("ws2v", "ws2g"))
    s2 = ring(
        5, "z", lambda i, h: ws2.at[:, i, pl.ds(h * quarter, quarter)],
        max(p2 + 0.1, s1 - 2.0), 11.2, nothing,
    )
    p3 = ring(6, "z", lambda i, h: wc2.at[i, y, rows_of(h, deep2)], s1 + 3.0, 3.0, loaded("wc2"))
    c2 = ring(
        7, "y", lambda i, h: wc2.at[pl.ds(h * quarter, quarter), i],
        max(p3 + 0.1, c1 - 2.0), 5.6, nothing,
    )

    def normalise():
        loads["raw"].wait()
        def body(i, carry):
            part = pl.ds(pl.multiple_of(i * 16, 16), 16)
            value = raw[part, :].astype(F32)
            scale = lax.rsqrt(jnp.mean(value * value, axis=1, keepdims=True) + 1e-6)
            normed[part, :] = (value * scale * norm_gain[...]).astype(BF)
            return carry
        lax.fori_loop(0, length // 16, body, 0)

    def spread():
        return ((iota((size, flat), 1) & (size - 1)) == iota((size, flat), 0)).astype(F32)

    def owner():
        return (iota((groups, flat), 1) // size) == iota((groups, flat), 0)

    def as_row(table):
        wide_table = jnp.dot(table, spread(), precision=HIGHEST, preferred_element_type=F32)
        return jnp.sum(jnp.where(owner(), wide_table, 0.0), axis=0, keepdims=True)

    def as_table(row):
        return lax.dot_general(
            jnp.where(owner(), row, 0.0), spread(), NT, precision=HIGHEST, preferred_element_type=F32
        )

    total_tokens = length * SIDE * SIDE

    def tables():
        rate = -as_row(decay_rate[...]) / total_tokens
        turn = as_row(frequency[...])
        rows[0:1, :] = as_row(initial_state[0])
        rows[1:2, :] = as_row(initial_state[1])
        magnitude = jnp.exp(rate)
        step_r = magnitude * jnp.cos(turn)
        step_i = magnitude * jnp.sin(turn)
        modulus = rate * rate + turn * turn
        lift = step_r - 1.0
        factor_r = (lift * rate + step_i * turn) / modulus
        factor_i = (step_i * rate - lift * turn) / modulus
        count = iota((8, flat), 0) + 1
        block_r, block_i = jnp.ones((8, flat), F32), jnp.zeros((8, flat), F32)
        square_r, square_i = step_r, step_i
        for place in range(4):
            chosen = ((count >> place) & 1) == 1
            next_r, next_i = rotate(block_r, block_i, square_r, square_i)
            block_r = jnp.where(chosen, next_r, block_r)
            block_i = jnp.where(chosen, next_i, block_i)
            if place < 3:
                square_r, square_i = rotate(square_r, square_i, square_r, square_i)
        rows[2:3, :], rows[3:4, :] = square_r, square_i
        rows[4:5, :], rows[5:6, :] = factor_r, factor_i

        def body(i, carry):
            now_r, now_i = carry
            part = pl.ds(pl.multiple_of(i * 8, 8), 8)
            power_r[part, :], power_i[part, :] = now_r, now_i
            inverse = 1.0 / (now_r * now_r + now_i * now_i)
            un_r, un_i = rotate(now_r * inverse, -now_i * inverse, rows[4:5, :], rows[5:6, :])
            undo_r[part, :], undo_i[part, :] = un_r, un_i
            return rotate(now_r, now_i, rows[2:3, :], rows[3:4, :])
        lax.fori_loop(0, length // 8, body, (block_r, block_i))

    def matrices():
        tile = ((iota((wide, width), 1) & (wide - 1)) == iota((wide, width), 0)).astype(BF)
        for source, dest in ((input_real, drive_r), (input_imag, drive_i)):
            for g in range(groups):
                copied = jnp.dot(source[g].astype(BF), tile, preferred_element_type=F32)
                kept = iota((size, width), 1) // wide == g
                dest[g * size:(g + 1) * size, :] = jnp.where(kept, copied, 0.0).astype(BF)
        stretch = spread().astype(BF)
        for part, (source, sign) in enumerate(((output_real, 1.0), (output_imag, -1.0))):
            for g in range(groups):
                copied = jnp.dot((sign * source[g]).astype(BF), stretch, preferred_element_type=F32)
                kept = iota((wide, flat), 1) // size == g
                emit[g * wide:(g + 1) * wide, part * flat:(part + 1) * flat] = (
                    jnp.where(kept, copied, 0.0).astype(BF)
                )

    at(13.0, normalise)
    at(13.5, tables)
    at(13.6, matrices)

    chunk = 256

    def recur():
        drive = jnp.dot(
            normed[...], ws1[...].reshape(normed.shape[1], width), preferred_element_type=F32
        ).astype(BF)
        feed[...] = drive
        for j in range(flat // chunk):
            part = slice(j * chunk, (j + 1) * chunk)
            shift = slice(flat + j * chunk, flat + (j + 1) * chunk)
            push_r = lax.dot_general(drive, drive_r[part, :], NT, preferred_element_type=F32)
            push_i = lax.dot_general(drive, drive_i[part, :], NT, preferred_element_type=F32)
            back_r, back_i = rotate(undo_r[:, part], undo_i[:, part], push_r, push_i)
            scaled[:, part] = back_r.astype(BF)
            scaled[:, shift] = back_i.astype(BF)
        lower = (iota((length, length), 0) >= iota((length, length), 1)).astype(BF)
        for j in range(2 * flat // chunk):
            part = slice(j * chunk, (j + 1) * chunk)
            summed[:, part] = jnp.dot(lower, scaled[:, part], preferred_element_type=F32)
        end_r, end_i = rotate(
            power_r[length - 1:length, :], power_i[length - 1:length, :],
            summed[length - 1:length, 0:flat], summed[length - 1:length, flat:2 * flat],
        )
        finals[y, :, 0:flat], finals[y, :, flat:2 * flat] = end_r, end_i
        for d in range(1, SIDE):
            moving = remote(
                finals.at[y], finals.at[y], scan_send.at[0, d - 1], scan_recv.at[0, d - 1],
                device(z, step_to(y, d, SIDE), t),
            )
            moving.start()
            sent.append(moving)

    def scan_row():
        for d in range(1, SIDE):
            source = step_to(y, -d, SIDE)
            remote(
                finals.at[source], finals.at[source], scan_send.at[0, d - 1],
                scan_recv.at[0, d - 1], device(z, source, t),
            ).wait_recv()
        span_r, span_i = power_r[length - 1:length, :], power_i[length - 1:length, :]
        zero = jnp.zeros((1, flat), F32)
        sum_r, sum_i, before_r, before_i = zero, zero, zero, zero
        jump_r, jump_i = zero + 1.0, zero
        mine_r, mine_i = zero, zero
        for yy in range(SIDE):
            before_r, before_i = jnp.where(y == yy, sum_r, before_r), jnp.where(y == yy, sum_i, before_i)
            mine_r, mine_i = jnp.where(y == yy, jump_r, mine_r), jnp.where(y == yy, jump_i, mine_i)
            next_r, next_i = rotate(span_r, span_i, sum_r, sum_i)
            sum_r = next_r + finals[yy, :, 0:flat]
            sum_i = next_i + finals[yy, :, flat:2 * flat]
            jump_r, jump_i = rotate(span_r, span_i, jump_r, jump_i)
        rows[6:7, :], rows[7:8, :] = before_r, before_i
        rows[8:9, :], rows[9:10, :] = mine_r, mine_i
        rows[10:11, :], rows[11:12, :] = jump_r, jump_i
        totals[z, :, 0:flat], totals[z, :, flat:2 * flat] = sum_r, sum_i
        for d in range(1, SIDE):
            moving = remote(
                totals.at[z], totals.at[z], scan_send.at[1, d - 1], scan_recv.at[1, d - 1],
                device(step_to(z, d, SIDE), y, t),
            )
            moving.start()
            sent.append(moving)

    def scan_all():
        for d in range(1, SIDE):
            source = step_to(z, -d, SIDE)
            remote(
                totals.at[source], totals.at[source], scan_send.at[1, d - 1],
                scan_recv.at[1, d - 1], device(source, y, t),
            ).wait_recv()
        sum_r, sum_i = rows[0:1, :], rows[1:2, :]
        jump_r, jump_i = rows[10:11, :], rows[11:12, :]
        start_r, start_i = sum_r, sum_i
        for zz in range(SIDE):
            start_r, start_i = jnp.where(z == zz, sum_r, start_r), jnp.where(z == zz, sum_i, start_i)
            next_r, next_i = rotate(jump_r, jump_i, sum_r, sum_i)
            sum_r = next_r + totals[zz, :, 0:flat]
            sum_i = next_i + totals[zz, :, flat:2 * flat]
        final_state[0] = as_table(sum_r)
        final_state[1] = as_table(sum_i)
        lead_r, lead_i = rotate(rows[8:9, :], rows[9:10, :], start_r, start_i)
        entry_r, entry_i = lead_r + rows[6:7, :], lead_i + rows[7:8, :]
        for j in range(flat // chunk):
            part = slice(j * chunk, (j + 1) * chunk)
            shift = slice(flat + j * chunk, flat + (j + 1) * chunk)
            state_r, state_i = rotate(
                power_r[:, part], power_i[:, part],
                summed[:, part] + entry_r[:, part], summed[:, shift] + entry_i[:, part],
            )
            states[:, part] = state_r.astype(BF)
            states[:, shift] = state_i.astype(BF)
        answer = lax.dot_general(states[...], emit[...], NT, preferred_element_type=F32)
        answer = answer + skip_gain[...] * feed[...].astype(F32)
        act_all[t] = jax.nn.gelu(answer).astype(BF)
        share(0, act_all)

    other = t + 1 - 2 * core

    def share(number, blocks):
        moving = remote(
            blocks.at[t], blocks.at[t], tp_send.at[number, 0], tp_recv.at[number, 0],
            device(z, y, other),
        )
        moving.start()
        sent.append(moving)
        for d in range(1, CHIPS):
            moving = remote(
                blocks.at[t], blocks.at[t], tp_send.at[number, d], tp_recv.at[number, d],
                device(z, y, step_to(chip, d, CHIPS) * 2 + core),
            )
            moving.start()
            sent.append(moving)

    def pass_on(number, blocks):
        for d in (1, 3, 2):
            source = step_to(chip, -d, CHIPS) * 2 + core
            remote(
                blocks.at[source], blocks.at[source], tp_send.at[number, d], tp_recv.at[number, d],
                device(z, y, source),
            ).wait_recv()
            moving = remote(
                blocks.at[source], blocks.at[source], tp_send.at[number, 3 + d],
                tp_recv.at[number, 3 + d], device(z, y, other),
            )
            moving.start()
            sent.append(moving)

    def shared(number, blocks):
        remote(
            blocks.at[other], blocks.at[other], tp_send.at[number, 0], tp_recv.at[number, 0],
            device(z, y, other),
        ).wait_recv()
        for d in (1, 3, 2):
            source = step_to(chip, -d, CHIPS) * 2 + 1 - core
            remote(
                blocks.at[source], blocks.at[source], tp_send.at[number, 3 + d],
                tp_recv.at[number, 3 + d], device(z, y, other),
            ).wait_recv()

    at(s1 + 0.1, recur)
    at(s1 + 11.0, scan_row)
    at(s1 + 21.0, scan_all)
    at(s1 + 30.0, lambda: pass_on(0, act_all))

    edge = halo.shape[0]
    kernel_size = conv_taps.shape[0]

    def gate():
        value_in = jnp.dot(
            normed[...], wc1[0].reshape(normed.shape[1], width), preferred_element_type=F32
        )
        gate_in = jnp.dot(
            normed[...], wc1[1].reshape(normed.shape[1], width), preferred_element_type=F32
        )
        gated[...] = (value_in * jax.nn.sigmoid(gate_in)).astype(BF)
        moving = remote(
            gated.at[pl.ds(length - edge, edge)], halo, halo_sem.at[0], halo_sem.at[1],
            {"sp": following, "tp": t},
        )
        moving.start()
        sent.append(moving)
        padded[edge:edge + length, :] = gated[...].astype(F32)

    def convolve():
        remote(
            gated.at[pl.ds(length - edge, edge)], halo, halo_sem.at[0], halo_sem.at[1],
            {"sp": preceding, "tp": t},
        ).wait_recv()
        padded[0:edge, :] = jnp.where(seq > 0, halo[...].astype(F32), 0.0)
        lag = edge - (kernel_size - 1)
        for lane in range(width // 128):
            lanes = slice(lane * 128, (lane + 1) * 128)
            answer = jnp.zeros((length, 128), F32)
            for b in range(8):
                tall = length + (8 if b else 0)
                part = jnp.zeros((tall, 128), F32)
                for a in range(edge // 8 + 1):
                    k = 8 * a + b - lag
                    if 0 <= k < kernel_size:
                        part = part + conv_taps[k:k + 1, lanes] * padded[8 * a:8 * a + tall, lanes]
                if b:
                    shifted[b, :, :] = part
                    answer = answer + shifted[b, b:b + length, :]
                else:
                    answer = answer + part
            conv_all[t, :, lanes] = answer.astype(BF)
        share(1, conv_all)

    def channel_norm():
        count = 2 * CHIPS * width
        def body(i, carry):
            part = pl.ds(pl.multiple_of(i * 16, 16), 16)
            pieces = [conv_all[c, part, :].astype(F32) for c in range(2 * CHIPS)]
            total = pieces[0]
            for piece in pieces[1:]:
                total = total + piece
            mean = jnp.sum(total, axis=1, keepdims=True) / count
            pieces = [piece - mean for piece in pieces]
            total = pieces[0] * pieces[0]
            for piece in pieces[1:]:
                total = total + piece * piece
            scale = lax.rsqrt(jnp.sum(total, axis=1, keepdims=True) / count + 1e-5)
            for c, piece in enumerate(pieces):
                lanes = slice(c * width, (c + 1) * width)
                value = piece * scale * chan_gain[:, lanes] + chan_shift[:, lanes]
                conv_act[c, part, :] = jax.nn.silu(value).astype(BF)
            return carry
        lax.fori_loop(0, length // 16, body, 0)

    at(c1 + 0.1, gate)
    at(c1 + 7.0, convolve)
    at(c1 + 15.0, lambda: pass_on(1, conv_all))
    at(c1 + 16.5, lambda: (shared(1, conv_all), channel_norm()))

    columns = out.shape[1]

    def project(blocks, weights, lanes):
        total = None
        for c in range(2 * CHIPS):
            term = jnp.dot(
                blocks[c], weights[c].reshape(width, columns)[:, lanes], preferred_element_type=F32
            )
            total = term if total is None else total + term
        return total

    def state_out():
        shared(0, act_all)
        for n in range(columns // 256):
            lanes = slice(n * 256, (n + 1) * 256)
            mixed[:, lanes] = project(act_all, ws2.at[0], lanes) * jax.nn.sigmoid(
                project(act_all, ws2.at[1], lanes)
            )

    def conv_out():
        for n in range(columns // 256):
            lanes = slice(n * 256, (n + 1) * 256)
            result[:, lanes] = (mixed[:, lanes] + project(conv_act, wc2, lanes)).astype(BF)
        moving = pltpu.make_async_copy(result, out, load_sem.at[7])
        moving.start()
        for copy in sent:
            copy.wait_send()
        moving.wait()

    at(s2 + 0.1, state_out)
    at(max(s2, c2) + 0.2, conv_out)

    for _, _, fn in sorted(events, key=lambda e: e[:2]):
        fn()


def local(
    tokens, norm_gain, conv_value, conv_gate, state_feed, conv_taps, chan_gain, chan_shift,
    conv_project, decay_rate, frequency, input_real, input_imag, output_real, output_imag,
    skip_gain, state_value, state_gate, initial_state,
):
    length, features = tokens.shape
    groups, size, wide = input_real.shape
    flat, width = groups * size, groups * wide
    deep1, columns = conv_value.shape[0], conv_project.shape[1]
    deep2 = conv_project.shape[0]
    edge = 32
    args = (
        tokens, norm_gain.reshape(1, -1), conv_value, conv_gate, state_feed, conv_taps,
        chan_gain.reshape(1, -1), chan_shift.reshape(1, -1), conv_project, decay_rate, frequency,
        input_real, input_imag, output_real, output_imag, skip_gain.reshape(1, -1), state_value,
        state_gate, initial_state,
    )
    large = {0, 2, 3, 4, 8, 16, 17}
    anywhere = pl.BlockSpec(memory_space=pl.ANY)
    held = pl.BlockSpec(memory_space=pltpu.VMEM)
    vmem = pltpu.VMEM
    dma = pltpu.SemaphoreType.DMA
    return pl.pallas_call(
        kernel,
        out_shape=(
            jax.ShapeDtypeStruct((length, columns), BF),
            jax.ShapeDtypeStruct(initial_state.shape, F32),
        ),
        in_specs=[anywhere if i in large else held for i in range(len(args))],
        out_specs=(anywhere, held),
        scratch_shapes=[
            vmem((SIDE, SIDE, deep1, width), BF),
            vmem((2, SIDE, SIDE, deep1, width), BF),
            vmem((2, SIDE, SIDE, deep2, columns), BF),
            vmem((SIDE, SIDE, deep2, columns), BF),
            vmem((length, features), BF),
            vmem((length, features), BF),
            vmem((length, columns), BF),
            vmem((length, flat), F32),
            vmem((length, flat), F32),
            vmem((length, flat), F32),
            vmem((length, flat), F32),
            vmem((flat, width), BF),
            vmem((flat, width), BF),
            vmem((width, 2 * flat), BF),
            vmem((length, width), BF),
            vmem((length, 2 * flat), BF),
            vmem((length, 2 * flat), F32),
            vmem((length, 2 * flat), BF),
            vmem((16, flat), F32),
            vmem((SIDE, 1, 2 * flat), F32),
            vmem((SIDE, 1, 2 * flat), F32),
            vmem((length, width), BF),
            vmem((edge, width), BF),
            vmem((edge + length, width), F32),
            vmem((8, length + 8, 128), F32),
            vmem((2 * CHIPS, length, width), BF),
            vmem((2 * CHIPS, length, width), BF),
            vmem((2 * CHIPS, length, width), BF),
            vmem((length, columns), F32),
            dma((8,)),
            dma((8, len(SLOTS))),
            dma((8, len(SLOTS))),
            dma((2, SIDE - 1)),
            dma((2, SIDE - 1)),
            dma((2,)),
            dma((2, 7)),
            dma((2, 7)),
        ],
        compiler_params=pltpu.CompilerParams(
            collective_id=0, has_side_effects=True, vmem_limit_bytes=60 * 1024 * 1024
        ),
        name="mixer",
    )(*args)


def solution(mesh):
    in_specs = (
        P("sp", None), P(), P("sp", "tp"), P("sp", "tp"), P("sp", "tp"), P(None, "tp"), P(), P(),
        P("sp", "tp"), P("tp", None), P("tp", None), P("tp", None, None), P("tp", None, None),
        P("tp", None, None), P("tp", None, None), P("tp"), P("sp", "tp"), P("sp", "tp"),
        P(None, "tp", None),
    )
    out_specs = (P("sp", "tp"), P(None, "tp", None))
    return jax.shard_map(local, mesh=mesh, in_specs=in_specs, out_specs=out_specs, check_vma=False)
```

time: 218 us -> 129 us (0.59)
  Pallas kernels: 0 us -> 122 us
  waiting for transfers between devices: 112 us -> 0 us
  other arithmetic: 40.3 us -> 0 us
  starting transfers between devices: 20 us -> 0 us
  matrix products: 19 us -> 0 us
  between operations: 16.4 us -> 0.64 us
  local copies, waits for them, and re-layouts: 9.94 us -> 6.76 us
    pallas_call x0 -> x1, Pallas kernels: none -> 122 us  [local(): pl.pallas_call(kernel, out_shape=(jax.ShapeDtypeStruct((length, columns),...]
    all_gather x2 -> x0, waiting for transfers between devices: 79.8 us -> none  [the longest x1 78 us: local(): lax.all_gather(in_block, 'sp', axis=0, tiled=True)]
    all_to_all x2 -> x0, waiting for transfers between devices: 27.8 us -> none  [copy_for_each(): lax.all_to_all(jnp.broadcast_to(shard[None], (length, *shard.shape)), axi...]
    dot_general x9 -> x0, matrix products: 19 us -> none  [the longest x1 4.6 us: local(): summed_imag = jnp.dot(lower, scaled_imag)]
    all_to_all x2 -> x0, starting transfers between devices: 16.8 us -> none  [copy_for_each(): lax.all_to_all(jnp.broadcast_to(shard[None], (length, *shard.shape)), axi...]
    add x6 -> x0, other arithmetic: 16.4 us -> none  [the longest x3 7.44 us: rotate(): first_real * second_imag + first_imag * second_real]
    select_n x6 -> x0, other arithmetic: 7.59 us -> none  [the longest x3 3.8 us: power_table(): result_real = jnp.where(chosen, next_real, result_real)]
    reduce_sum x7 -> x0, other arithmetic: 4.94 us -> none  [the longest x1 1.72 us: local(): final_imag = closing_imag + jnp.sum(carried_imag, axis=0)]
  transfers between devices with their start and end apart: 5 -> 0, of which waited for: 5 -> 0; matrix products, arithmetic and copies ran while one was open for 27% -> 0% of each run, Pallas kernels for 0% -> 0%
where the time goes in v1:
time: 129 us
  Pallas kernels  122 us (95%)
  local copies, waits for them, and re-layouts  6.76 us (5%)
    pallas_call x1, Pallas kernels, local(): pl.pallas_call(kernel, out_shape=(jax.ShapeDtypeStruct((length, columns),...  122 us
    unnamed x4, local copies, waits for them, and re-layouts  6.76 us

profile of v1, /device:TPU:1, one launch (start us, length us, event | category | flops | bytes accessed | tf_op | source)
XLA Modules:
  0.0 128.9 jit_solution(15609118048885542843)
XLA Ops:
  0.6 1.9 %copy.21.input_real = f32[16,64,16]{2,1,0:T(8,128)} copy(f32[16,64,16]{1,2,0:T(8,128)} %param.30) | data formatting | bytes 131072 | tf_op args[11]
  2.5 1.9 %copy.22.input_imag = f32[16,64,16]{2,1,0:T(8,128)} copy(f32[16,64,16]{1,2,0:T(8,128)} %param.31) | data formatting | bytes 131072 | tf_op args[12]
  4.5 121.5 %mixer.1 = (bf16[192,512]{1,0:T(8,128)(2,1)}, f32[2,16,64]{2,1,0:T(8,128)}) custom-call(bf16[192,4096]{1,0:T(8,128)(2,1)} %tokens.1, f32[1,4096]{1,0:T(1,128)} %bitcast.4, bf16[64,256]{1,0:T(8,128)(2,1)} %conv_value.1, bf16[64,256]{1,0:T(8,128)(2,1)} %conv_gate.1, bf16[64,256]{1,0:T(8,128)(2,1)} %state_feed.1, f32[31,256]{1,0:T(8,128)} %conv_taps.1, ...), custom_call_target="tpu_custom_call" | custom-call | tf_op jit(solution)/shard_map/mixer/pallas_call | solution.py:533
  126.0 1.6 %copy.25 = bf16[192,512]{1,0:T(8,128)(2,1)} copy(bf16[192,512]{1,0:T(8,128)(2,1)} %get-tuple-element.4) | data formatting | bytes 393216
  127.6 1.3 %copy.26 = f32[2,16,64]{2,1,0:T(8,128)} copy(f32[2,16,64]{2,1,0:T(8,128)} %get-tuple-element.5) | data formatting | bytes 16384

commit v2 on v1

--- a/solution.py
+++ b/solution.py
@@ -1,3 +1,5 @@
+import heapq
+
 import jax
 import jax.numpy as jnp
 from jax import lax
@@ -52,7 +54,7 @@
     z, y = seq // SIDE, seq % SIDE
     chip, core = t // 2, t % 2
     length = tokens.shape[0]
-    groups, size, wide = input_real.shape
+    groups, wide, size = input_real.shape
     flat = groups * size
     width = groups * wide
 
@@ -67,11 +69,35 @@
             src_ref=src, dst_ref=dst, send_sem=send, recv_sem=recv, device_id=to, device_id_type=MESH
         )
 
-    events = []
+    queue = []
     sent = []
-
-    def at(time, fn):
-        events.append((time, len(events), fn))
+    free = {}
+    clock = [0.0, 0]
+
+    def at(time, fn, cost=0.0):
+        heapq.heappush(queue, (time, clock[1], cost, fn))
+        clock[1] += 1
+
+    def run():
+        while queue:
+            time, _, cost, fn = heapq.heappop(queue)
+            clock[0] = max(clock[0], time)
+            fn()
+            clock[0] += cost
+
+    def transit(link, size, count=1, rate=46.6e3):
+        begin = max(clock[0], free.get(link, 0.0))
+        free[link] = begin + size * count / rate
+        return free[link] + 0.95 + 0.75 * count
+
+    def when_all(number, fn):
+        left = [number]
+
+        def one():
+            left[0] -= 1
+            if left[0] == 0:
+                fn()
+        return one
 
     loads = {}
 
@@ -103,78 +129,137 @@
         pl.semaphore_signal(barrier, inc=1, device_id=partner, device_id_type=MESH)
     pl.semaphore_wait(barrier, len(partners))
 
-    def ring(number, axis, block, start, tau, ready):
+    def beside(axis, by):
+        moved = step_to(here[axis], by, SIDE)
+        return device(moved, y, t) if axis == "z" else device(z, moved, t)
+
+    def ring(number, axis, block, size, done, nearly=None):
         position = here[axis]
-
-        def neighbour(direction):
-            beside = step_to(position, direction, SIDE)
-            return device(beside, y, t) if axis == "z" else device(z, beside, t)
+        finished = when_all(len(SLOTS), done)
+        passed = when_all(len(SLOTS) - 4, nearly or (lambda: None))
 
         def copy(direction, half, k, source):
             slot = SLOT_OF[(direction, half, k)]
             return remote(
                 block(source, half), block(source, half),
-                ring_send.at[number, slot], ring_recv.at[number, slot], neighbour(direction),
+                ring_send.at[number, slot], ring_recv.at[number, slot], beside(axis, direction),
             )
 
         def send(direction, half, k):
             moving = copy(direction, half, k, step_to(position, -direction * k, SIDE))
             moving.start()
             sent.append(moving)
-
-        def first():
-            ready()
-            for half in (0, 1):
-                for direction in (1, -1):
-                    send(direction, half, 0)
-
-        at(start, first)
+            time = transit((axis, direction), size)
+            at(time, lambda: arrived(direction, half, k))
 
         def arrived(direction, half, k):
             source = step_to(position, -direction * (k + 1), SIDE)
             copy(direction, half, k, source).wait_recv()
             if k + 1 < hops(direction, half):
                 send(direction, half, k + 1)
-
-        last = start
-        for k in range(SIDE // 2):
+                passed()
+            finished()
+
+        def first():
             for half in (0, 1):
                 for direction in (1, -1):
-                    if k < hops(direction, half):
-                        time = start + tau * k + (half + 1) * tau / 2 + 1.7
-                        last = max(last, time)
-                        at(time, lambda a=direction, b=half, c=k: arrived(a, b, c))
-        return last
-
-    def nothing():
-        pass
-
-    def loaded(*names):
-        def wait():
-            for name in names:
-                loads[name].wait()
-        return wait
+                    send(direction, half, 0)
+        return first
+
+    def spread_out(sems, axis, block, size, done):
+        position = here[axis]
+        finished = when_all(SIDE - 1, done)
+
+        def copy(d, source, to):
+            return remote(block(source), block(source), sems[0](d), sems[1](d), to)
+
+        def arrived(d):
+            copy(d, step_to(position, -d, SIDE), beside(axis, -d)).wait_recv()
+            finished()
+
+        def first():
+            for d in (4, 3, 5, 2, 6, 1, 7):
+                moving = copy(d, position, beside(axis, d))
+                moving.start()
+                sent.append(moving)
+                direction, count = (1, d) if d <= SIDE // 2 else (-1, SIDE - d)
+                time = transit((axis, direction), size, count)
+                at(time, lambda d=d: arrived(d))
+        return first
 
     quarter = SIDE // 2
     deep1, deep2 = ws1.shape[2] // 2, wc2.shape[2] // 2
+    piece = ws1.shape[2] * ws1.shape[3] * 2
 
     def rows_of(half, deep):
         return pl.ds(half * deep, deep)
 
-    ring(0, "y", lambda i, h: ws1.at[z, i, rows_of(h, deep1)], 0.0, 0.8, loaded("ws1"))
-    ring(1, "z", lambda i, h: wc1.at[h, i, y], 0.1, 1.4, loaded("wc1v", "wc1g"))
-    s1 = ring(2, "z", lambda i, h: ws1.at[i, pl.ds(h * quarter, quarter)], 9.0, 5.6, nothing)
-    c1 = ring(3, "y", lambda i, h: wc1.at[:, pl.ds(h * quarter, quarter), i], 12.5, 11.2, nothing)
-    p2 = ring(4, "y", lambda i, h: ws2.at[h, z, i], 15.0, 3.0, loaded("ws2v", "ws2g"))
-    s2 = ring(
-        5, "z", lambda i, h: ws2.at[:, i, pl.ds(h * quarter, quarter)],
-        max(p2 + 0.1, s1 - 2.0), 11.2, nothing,
-    )
-    p3 = ring(6, "z", lambda i, h: wc2.at[i, y, rows_of(h, deep2)], s1 + 3.0, 3.0, loaded("wc2"))
-    c2 = ring(
-        7, "y", lambda i, h: wc2.at[pl.ds(h * quarter, quarter), i],
-        max(p3 + 0.1, c1 - 2.0), 5.6, nothing,
-    )
+    def after(*names):
+        for name in names:
+            loads[name].wait()
+
+    def direct(number):
+        return (
+            lambda d: ring_send.at[number, d],
+            lambda d: ring_recv.at[number, d],
+        )
+
+    def both(fn):
+        return when_all(2, fn)
+
+    state_in = ring(
+        0, "z", lambda i, h: ws1.at[i, pl.ds(h * quarter, quarter)], 4 * piece,
+        lambda: at(clock[0], recur, 1.8), lambda: go_sv(),
+    )
+    sv_big = ring(
+        1, "z", lambda i, h: ws2.at[0, i, pl.ds(h * quarter, quarter)], 4 * piece,
+        lambda: state_ready(), lambda: go_sg(),
+    )
+    sg_big = ring(
+        2, "z", lambda i, h: ws2.at[1, i, pl.ds(h * quarter, quarter)], 4 * piece,
+        lambda: state_ready(),
+    )
+    go_sv, go_sg = both(sv_big), both(sg_big)
+    sg_small = ring(
+        3, "y", lambda i, h: ws2.at[1, z, i, rows_of(h, deep2)], piece / 2, lambda: go_sg()
+    )
+    sv_small = ring(
+        4, "y", lambda i, h: ws2.at[0, z, i, rows_of(h, deep2)], piece / 2,
+        lambda: (go_sv(), sg_small()),
+    )
+    conv_in = ring(
+        5, "y", lambda i, h: wc1.at[0, pl.ds(h * quarter, quarter), i], 4 * piece,
+        lambda: gate_ready(), lambda: go_cg(),
+    )
+    cg_big = ring(
+        6, "y", lambda i, h: wc1.at[1, pl.ds(h * quarter, quarter), i], 4 * piece,
+        lambda: gate_ready(), lambda: go_cp(),
+    )
+    cp_big = ring(
+        7, "y", lambda i, h: wc2.at[pl.ds(h * quarter, quarter), i], 4 * piece,
+        lambda: conv_ready(),
+    )
+    go_cg, go_cp = both(cg_big), both(cp_big)
+    cp_small = ring(
+        8, "z", lambda i, h: wc2.at[i, y, rows_of(h, deep2)], piece / 2, lambda: go_cp()
+    )
+    cg_small = ring(
+        9, "z", lambda i, h: wc1.at[1, i, y, rows_of(h, deep1)], piece / 2,
+        lambda: (go_cg(), cp_small()),
+    )
+    sf_small = spread_out(direct(10), "y", lambda i: ws1.at[z, i], piece, state_in)
+    cv_small = spread_out(direct(11), "z", lambda i: wc1.at[0, i, y], piece, conv_in)
+
+    def begin():
+        after("ws1")
+        sf_small()
+        after("wc1v")
+        cv_small()
+        after("wc1g")
+        cg_small()
+
+    at(0.0, begin)
+    at(5.0, lambda: (after("ws2v", "ws2g", "wc2"), sv_small()))
 
     def normalise():
         loads["raw"].wait()
@@ -239,24 +324,20 @@
         lax.fori_loop(0, length // 8, body, (block_r, block_i))
 
     def matrices():
-        tile = ((iota((wide, width), 1) & (wide - 1)) == iota((wide, width), 0)).astype(BF)
-        for source, dest in ((input_real, drive_r), (input_imag, drive_i)):
-            for g in range(groups):
-                copied = jnp.dot(source[g].astype(BF), tile, preferred_element_type=F32)
-                kept = iota((size, width), 1) // wide == g
-                dest[g * size:(g + 1) * size, :] = jnp.where(kept, copied, 0.0).astype(BF)
         stretch = spread().astype(BF)
-        for part, (source, sign) in enumerate(((output_real, 1.0), (output_imag, -1.0))):
+        def fill(source, sign, dest, lanes):
             for g in range(groups):
                 copied = jnp.dot((sign * source[g]).astype(BF), stretch, preferred_element_type=F32)
                 kept = iota((wide, flat), 1) // size == g
-                emit[g * wide:(g + 1) * wide, part * flat:(part + 1) * flat] = (
-                    jnp.where(kept, copied, 0.0).astype(BF)
-                )
-
-    at(13.0, normalise)
-    at(13.5, tables)
-    at(13.6, matrices)
+                dest[g * wide:(g + 1) * wide, lanes] = jnp.where(kept, copied, 0.0).astype(BF)
+        fill(input_real, 1.0, drive_r, slice(0, flat))
+        fill(input_imag, 1.0, drive_i, slice(0, flat))
+        fill(output_real, 1.0, emit, slice(0, flat))
+        fill(output_imag, -1.0, emit, slice(flat, 2 * flat))
+
+    at(8.0, normalise, 1.8)
+    at(9.0, tables, 1.4)
+    at(11.0, matrices, 1.0)
 
     chunk = 256
 
@@ -268,8 +349,8 @@
         for j in range(flat // chunk):
             part = slice(j * chunk, (j + 1) * chunk)
             shift = slice(flat + j * chunk, flat + (j + 1) * chunk)
-            push_r = lax.dot_general(drive, drive_r[part, :], NT, preferred_element_type=F32)
-            push_i = lax.dot_general(drive, drive_i[part, :], NT, preferred_element_type=F32)
+            push_r = jnp.dot(drive, drive_r[:, part], preferred_element_type=F32)
+            push_i = jnp.dot(drive, drive_i[:, part], preferred_element_type=F32)
             back_r, back_i = rotate(undo_r[:, part], undo_i[:, part], push_r, push_i)
             scaled[:, part] = back_r.astype(BF)
             scaled[:, shift] = back_i.astype(BF)
@@ -282,21 +363,17 @@
             summed[length - 1:length, 0:flat], summed[length - 1:length, flat:2 * flat],
         )
         finals[y, :, 0:flat], finals[y, :, flat:2 * flat] = end_r, end_i
-        for d in range(1, SIDE):
-            moving = remote(
-                finals.at[y], finals.at[y], scan_send.at[0, d - 1], scan_recv.at[0, d - 1],
-                device(z, step_to(y, d, SIDE), t),
-            )
-            moving.start()
-            sent.append(moving)
+        spread_out(
+            scan_sems(0), "y", lambda i: finals.at[i], 8 * flat, lambda: at(clock[0], scan_row, 0.1)
+        )()
+
+    def scan_sems(number):
+        return (
+            lambda d: scan_send.at[number, d - 1],
+            lambda d: scan_recv.at[number, d - 1],
+        )
 
     def scan_row():
-        for d in range(1, SIDE):
-            source = step_to(y, -d, SIDE)
-            remote(
-                finals.at[source], finals.at[source], scan_send.at[0, d - 1],
-                scan_recv.at[0, d - 1], device(z, source, t),
-            ).wait_recv()
         span_r, span_i = power_r[length - 1:length, :], power_i[length - 1:length, :]
         zero = jnp.zeros((1, flat), F32)
         sum_r, sum_i, before_r, before_i = zero, zero, zero, zero
@@ -313,21 +390,11 @@
         rows[8:9, :], rows[9:10, :] = mine_r, mine_i
         rows[10:11, :], rows[11:12, :] = jump_r, jump_i
         totals[z, :, 0:flat], totals[z, :, flat:2 * flat] = sum_r, sum_i
-        for d in range(1, SIDE):
-            moving = remote(
-                totals.at[z], totals.at[z], scan_send.at[1, d - 1], scan_recv.at[1, d - 1],
-                device(step_to(z, d, SIDE), y, t),
-            )
-            moving.start()
-            sent.append(moving)
+        spread_out(
+            scan_sems(1), "z", lambda i: totals.at[i], 8 * flat, lambda: at(clock[0], scan_all, 2.5)
+        )()
 
     def scan_all():
-        for d in range(1, SIDE):
-            source = step_to(z, -d, SIDE)
-            remote(
-                totals.at[source], totals.at[source], scan_send.at[1, d - 1],
-                scan_recv.at[1, d - 1], device(source, y, t),
-            ).wait_recv()
         sum_r, sum_i = rows[0:1, :], rows[1:2, :]
         jump_r, jump_i = rows[10:11, :], rows[11:12, :]
         start_r, start_i = sum_r, sum_i
@@ -352,55 +419,41 @@
         answer = lax.dot_general(states[...], emit[...], NT, preferred_element_type=F32)
         answer = answer + skip_gain[...] * feed[...].astype(F32)
         act_all[t] = jax.nn.gelu(answer).astype(BF)
-        share(0, act_all)
+        share(0, act_all, lambda: state_ready())
 
     other = t + 1 - 2 * core
 
-    def share(number, blocks):
-        moving = remote(
-            blocks.at[t], blocks.at[t], tp_send.at[number, 0], tp_recv.at[number, 0],
-            device(z, y, other),
-        )
-        moving.start()
-        sent.append(moving)
-        for d in range(1, CHIPS):
-            moving = remote(
-                blocks.at[t], blocks.at[t], tp_send.at[number, d], tp_recv.at[number, d],
-                device(z, y, step_to(chip, d, CHIPS) * 2 + core),
+    def share(number, blocks, done):
+        finished = when_all(4, done)
+        size = length * width * 2
+
+        def copy(slot, source, to):
+            return remote(
+                blocks.at[source], blocks.at[source], tp_send.at[number, slot],
+                tp_recv.at[number, slot], device(z, y, to),
             )
+
+        def start(moving):
             moving.start()
             sent.append(moving)
 
-    def pass_on(number, blocks):
-        for d in (1, 3, 2):
+        def near(d):
+            source = other if d == 0 else step_to(chip, -d, CHIPS) * 2 + 1 - core
+            copy(3 + d if d else 0, source, other).wait_recv()
+            finished()
+
+        def far(d):
             source = step_to(chip, -d, CHIPS) * 2 + core
-            remote(
-                blocks.at[source], blocks.at[source], tp_send.at[number, d], tp_recv.at[number, d],
-                device(z, y, source),
-            ).wait_recv()
-            moving = remote(
-                blocks.at[source], blocks.at[source], tp_send.at[number, 3 + d],
-                tp_recv.at[number, 3 + d], device(z, y, other),
-            )
-            moving.start()
-            sent.append(moving)
-
-    def shared(number, blocks):
-        remote(
-            blocks.at[other], blocks.at[other], tp_send.at[number, 0], tp_recv.at[number, 0],
-            device(z, y, other),
-        ).wait_recv()
-        for d in (1, 3, 2):
-            source = step_to(chip, -d, CHIPS) * 2 + 1 - core
-            remote(
-                blocks.at[source], blocks.at[source], tp_send.at[number, 3 + d],
-                tp_recv.at[number, 3 + d], device(z, y, other),
-            ).wait_recv()
-
-    at(s1 + 0.1, recur)
-    at(s1 + 11.0, scan_row)
-    at(s1 + 21.0, scan_all)
-    at(s1 + 30.0, lambda: pass_on(0, act_all))
+            copy(d, source, source).wait_recv()
+            start(copy(3 + d, source, other))
+            at(transit("core", size, 1, 300e3), lambda: near(d))
+
+        for d in (2, 1, 3):
+            start(copy(d, t, step_to(chip, d, CHIPS) * 2 + core))
+            time = transit(("x", -1 if d == 3 else 1), size, 2 if d == 2 else 1)
+            at(time, lambda d=d: far(d))
+        start(copy(0, t, other))
+        at(transit("core", size, 1, 300e3), lambda: near(0))
 
     edge = halo.shape[0]
     kernel_size = conv_taps.shape[0]
@@ -419,6 +472,7 @@
         )
         moving.start()
         sent.append(moving)
+        at(transit(("y", 1), edge * width * 2), convolve, 0.7)
         padded[edge:edge + length, :] = gated[...].astype(F32)
 
     def convolve():
@@ -444,7 +498,7 @@
                 else:
                     answer = answer + part
             conv_all[t, :, lanes] = answer.astype(BF)
-        share(1, conv_all)
+        share(1, conv_all, lambda: at(clock[0], channel_norm, 2.0))
 
     def channel_norm():
         count = 2 * CHIPS * width
@@ -466,11 +520,7 @@
                 conv_act[c, part, :] = jax.nn.silu(value).astype(BF)
             return carry
         lax.fori_loop(0, length // 16, body, 0)
-
-    at(c1 + 0.1, gate)
-    at(c1 + 7.0, convolve)
-    at(c1 + 15.0, lambda: pass_on(1, conv_all))
-    at(c1 + 16.5, lambda: (shared(1, conv_all), channel_norm()))
+        conv_ready()
 
     columns = out.shape[1]
 
@@ -484,12 +534,12 @@
         return total
 
     def state_out():
-        shared(0, act_all)
         for n in range(columns // 256):
             lanes = slice(n * 256, (n + 1) * 256)
             mixed[:, lanes] = project(act_all, ws2.at[0], lanes) * jax.nn.sigmoid(
                 project(act_all, ws2.at[1], lanes)
             )
+        conv_ready()
 
     def conv_out():
         for n in range(columns // 256):
@@ -501,11 +551,10 @@
             copy.wait_send()
         moving.wait()
 
-    at(s2 + 0.1, state_out)
-    at(max(s2, c2) + 0.2, conv_out)
-
-    for _, _, fn in sorted(events, key=lambda e: e[:2]):
-        fn()
+    state_ready = when_all(3, lambda: at(clock[0], state_out, 1.4))
+    gate_ready = both(lambda: at(clock[0], gate, 1.0))
+    conv_ready = when_all(3, lambda: at(clock[0], conv_out, 1.4))
+    run()
 
 
 def local(
@@ -522,7 +571,8 @@
     args = (
         tokens, norm_gain.reshape(1, -1), conv_value, conv_gate, state_feed, conv_taps,
         chan_gain.reshape(1, -1), chan_shift.reshape(1, -1), conv_project, decay_rate, frequency,
-        input_real, input_imag, output_real, output_imag, skip_gain.reshape(1, -1), state_value,
+        jnp.swapaxes(input_real, 1, 2), jnp.swapaxes(input_imag, 1, 2), output_real, output_imag,
+        skip_gain.reshape(1, -1), state_value,
         state_gate, initial_state,
     )
     large = {0, 2, 3, 4, 8, 16, 17}
@@ -550,8 +600,8 @@
             vmem((length, flat), F32),
             vmem((length, flat), F32),
             vmem((length, flat), F32),
-            vmem((flat, width), BF),
-            vmem((flat, width), BF),
+            vmem((width, flat), BF),
+            vmem((width, flat), BF),
             vmem((width, 2 * flat), BF),
             vmem((length, width), BF),
             vmem((length, 2 * flat), BF),
@@ -569,8 +619,8 @@
             vmem((2 * CHIPS, length, width), BF),
             vmem((length, columns), F32),
             dma((8,)),
-            dma((8, len(SLOTS))),
-            dma((8, len(SLOTS))),
+            dma((12, len(SLOTS))),
+            dma((12, len(SLOTS))),
             dma((2, SIDE - 1)),
             dma((2, SIDE - 1)),
             dma((2,)),

time: 129 us -> 113 us (0.88)
  Pallas kernels: 122 us -> 109 us
  local copies, waits for them, and re-layouts: 6.76 us -> 2.94 us
    pallas_call x1, Pallas kernels: 122 us -> 109 us  [local(): pl.pallas_call(kernel, out_shape=(jax.ShapeDtypeStruct((length, columns),...]
    unnamed x4 -> x2, local copies, waits for them, and re-layouts: 6.76 us -> 2.94 us
where the time goes in v2:
time: 113 us; the launch traced here: 112 us
  Pallas kernels  109 us (96%)
  local copies, waits for them, and re-layouts  2.94 us (3%)
    pallas_call x1, Pallas kernels, local(): pl.pallas_call(kernel, out_shape=(jax.ShapeDtypeStruct((length, columns),...  109 us
    unnamed x2, local copies, waits for them, and re-layouts  2.94 us

profile of v2, /device:TPU:1, one launch (start us, length us, event | category | flops | bytes accessed | tf_op | source)
XLA Modules:
  0.0 112.4 jit_solution(30180564115742922)
XLA Ops:
  0.6 108.8 %mixer.1 = (bf16[192,512]{1,0:T(8,128)(2,1)}, f32[2,16,64]{2,1,0:T(8,128)}) custom-call(bf16[192,4096]{1,0:T(8,128)(2,1)} %tokens.1, f32[1,4096]{1,0:T(1,128)} %bitcast.8, bf16[64,256]{1,0:T(8,128)(2,1)} %conv_value.1, bf16[64,256]{1,0:T(8,128)(2,1)} %conv_gate.1, bf16[64,256]{1,0:T(8,128)(2,1)} %state_feed.1, f32[31,256]{1,0:T(8,128)} %conv_taps.1, ...), custom_call_target="tpu_custom_call" | custom-call | tf_op jit(solution)/shard_map/mixer/pallas_call | solution.py:583
  109.4 1.6 %copy.23 = bf16[192,512]{1,0:T(8,128)(2,1)} copy(bf16[192,512]{1,0:T(8,128)(2,1)} %get-tuple-element.4) | data formatting | bytes 393216
  111.1 1.3 %copy.24 = f32[2,16,64]{2,1,0:T(8,128)} copy(f32[2,16,64]{2,1,0:T(8,128)} %get-tuple-element.5) | data formatting | bytes 16384

commit v3 on v2

--- a/solution.py
+++ b/solution.py
@@ -39,16 +39,25 @@
     return lax.broadcasted_iota(jnp.int32, shape, dim)
 
 
-def kernel(
-    tokens, norm_gain, conv_value, conv_gate, state_feed, conv_taps, chan_gain, chan_shift,
-    conv_project, decay_rate, frequency, input_real, input_imag, output_real, output_imag,
-    skip_gain, state_value, state_gate, initial_state,
-    out, final_state,
-    ws1, wc1, ws2, wc2, raw, normed, result,
-    power_r, power_i, undo_r, undo_i, drive_r, drive_i, emit, feed, scaled, summed, states,
-    rows, finals, totals, gated, halo, padded, shifted, conv_all, act_all, conv_act, mixed,
-    load_sem, ring_send, ring_recv, scan_send, scan_recv, halo_sem, tp_send, tp_recv,
-):
+SMALL = (1, 5, 6, 7, 9, 10, 11, 12, 13, 14, 15, 18)
+
+
+def kernel(*refs):
+    (
+        tokens, norm_gain, conv_value, conv_gate, state_feed, conv_taps, chan_gain, chan_shift,
+        conv_project, decay_rate, frequency, input_real, input_imag, output_real, output_imag,
+        skip_gain, state_value, state_gate, initial_state, out, final_out,
+    ) = refs[:21]
+    small = refs[21:21 + len(SMALL)]
+    (
+        ws1, wc1, ws2, wc2, stage_s1, stage_c1, stage_s2, stage_c2, raw, scale, normed, result,
+        final_state, power_r, power_i, undo_r, undo_i, drive_r, drive_i, emit, feed, scaled, summed,
+        states, rows, finals, totals, feed_half, feed_back, gated_half, gated_back, halo, padded,
+        shifted, conv_all, act_all, conv_act, state_half, state_back, state_got, conv_half, conv_back,
+        conv_got,
+        load_sem, ring_send, ring_recv, scan_send, scan_recv, halo_sem, tp_send, tp_recv, pair_send,
+        pair_recv,
+    ) = refs[21 + len(SMALL):]
     seq = lax.axis_index("sp")
     t = lax.axis_index("tp")
     z, y = seq // SIDE, seq % SIDE
@@ -57,6 +66,9 @@
     groups, wide, size = input_real.shape
     flat = groups * size
     width = groups * wide
+    part_width = width // 2
+    columns = out.shape[1]
+    part_columns = columns // 2
 
     def device(zz, yy, tt):
         return {"sp": zz * SIDE + yy, "tp": tt}
@@ -85,6 +97,19 @@
             fn()
             clock[0] += cost
 
+    def start(moving):
+        moving.start()
+        sent.append((clock[0], moving))
+
+    def drain(before):
+        kept = []
+        for time, moving in sent:
+            if time < before:
+                moving.wait_send()
+            else:
+                kept.append((time, moving))
+        sent[:] = kept
+
     def transit(link, size, count=1, rate=46.6e3):
         begin = max(clock[0], free.get(link, 0.0))
         free[link] = begin + size * count / rate
@@ -99,22 +124,50 @@
                 fn()
         return one
 
-    loads = {}
-
-    def load(name, index, src, dst):
-        loads[name] = pltpu.make_async_copy(src, dst, load_sem.at[index])
-        loads[name].start()
-
-    load("ws1", 0, state_feed, ws1.at[z, y])
-    load("wc1v", 1, conv_value, wc1.at[0, z, y])
-    load("wc1g", 2, conv_gate, wc1.at[1, z, y])
-    load("ws2v", 3, state_value, ws2.at[0, z, y])
-    load("ws2g", 4, state_gate, ws2.at[1, z, y])
-    load("wc2", 5, conv_project, wc2.at[z, y])
-    load("raw", 6, tokens, raw)
+    loads, counted = {}, []
+
+    def load(name, src, dst):
+        moving = pltpu.make_async_copy(src, dst, load_sem.at[len(counted)])
+        moving.start()
+        counted.append(name)
+        loads.setdefault(name, []).append(moving)
+
+    def after(*names):
+        for name in names:
+            for moving in loads.pop(name, []):
+                moving.wait()
+
+    here = {"z": z, "y": y}
+    odd = {"z": z % 2, "y": y % 2}
+
+    def lanes_from(half, count):
+        return pl.ds(pl.multiple_of(half * count, count), count)
+
+    def staged(name, axis, pieces, stage, own, count):
+        for half in (0, 1):
+            for i, source in enumerate(pieces):
+                load(
+                    name, source.at[:, half * count:(half + 1) * count],
+                    stage.at[half, :, i * count:(i + 1) * count],
+                )
+        for i, source in enumerate(pieces):
+            load(
+                name, source.at[:, lanes_from(odd[axis], count)], own.at[:, i * count:(i + 1) * count]
+            )
+
+    staged("s1", "y", (state_feed,), stage_s1, ws1.at[z, y], part_width)
+    staged("c1", "z", (conv_value, conv_gate), stage_c1, wc1.at[z, y], part_width)
+    load("raw", tokens, raw)
+    for i, place in enumerate(SMALL):
+        load("small", refs[place], small[i])
+    (
+        norm_gain, conv_taps, chan_gain, chan_shift, decay_rate, frequency, input_real, input_imag,
+        output_real, output_imag, skip_gain, initial_state,
+    ) = small
+    staged("s2", "y", (state_value, state_gate), stage_s2, ws2.at[z, y], part_columns)
+    staged("c2", "z", (conv_project,), stage_c2, wc2.at[z, y], part_columns)
 
     barrier = pltpu.get_barrier_semaphore()
-    here = {"z": z, "y": y}
     following = lax.rem(seq + 1, SIDE * SIDE)
     preceding = lax.rem(seq + SIDE * SIDE - 1, SIDE * SIDE)
     partners = []
@@ -147,8 +200,7 @@
 
         def send(direction, half, k):
             moving = copy(direction, half, k, step_to(position, -direction * k, SIDE))
-            moving.start()
-            sent.append(moving)
+            start(moving)
             time = transit((axis, direction), size)
             at(time, lambda: arrived(direction, half, k))
 
@@ -180,96 +232,162 @@
         def first():
             for d in (4, 3, 5, 2, 6, 1, 7):
                 moving = copy(d, position, beside(axis, d))
-                moving.start()
-                sent.append(moving)
+                start(moving)
                 direction, count = (1, d) if d <= SIDE // 2 else (-1, SIDE - d)
                 time = transit((axis, direction), size, count)
                 at(time, lambda d=d: arrived(d))
         return first
 
+    def deal(number, axis, stage, block, size, done):
+        position = here[axis]
+        finished = when_all(SIDE - 1, done)
+
+        def copy(d, source, to):
+            half = odd[axis] if d % 2 == 0 else 1 - odd[axis]
+            return remote(
+                stage.at[half], block(source), ring_send.at[number, d], ring_recv.at[number, d], to
+            )
+
+        def arrived(d):
+            copy(d, step_to(position, -d, SIDE), beside(axis, -d)).wait_recv()
+            finished()
+
+        def first():
+            for d in (4, 3, 5, 2, 6, 1, 7):
+                start(copy(d, position, beside(axis, d)))
+                direction, count = (1, d) if d <= SIDE // 2 else (-1, SIDE - d)
+                time = transit((axis, direction), size, count)
+                at(time, lambda d=d: arrived(d))
+        return first
+
+    def mate(axis):
+        other_one = here[axis] + 1 - 2 * odd[axis]
+        return device(other_one, y, t) if axis == "z" else device(z, other_one, t)
+
+    def hand_over(number, axis, src, dst, landing, size, done):
+        start(remote(src, dst, pair_send.at[number], pair_recv.at[number], mate(axis)))
+        time = max(transit((axis, 1), size), transit((axis, -1), size))
+
+        def arrived():
+            remote(src, landing, pair_send.at[number], pair_recv.at[number], mate(axis)).wait_recv()
+            done()
+        at(time, arrived)
+
+    other = t + 1 - 2 * core
+
+    def share(number, block, tall, size, done):
+        finished = when_all(5, done)
+        halves = (pl.ds(0, tall // 2), pl.ds(tall // 2, tall // 2))
+        whole = pl.ds(0, tall)
+
+        def copy(slot, source, part, to):
+            return remote(
+                block(source).at[part], block(source).at[part], tp_send.at[number, slot],
+                tp_recv.at[number, slot], device(z, y, to),
+            )
+
+        def from_chip(d, which):
+            return step_to(chip, -d, CHIPS) * 2 + which
+
+        def near(slot, source, part):
+            copy(slot, source, part, other).wait_recv()
+            finished()
+
+        def to_core(slot, d, part, amount):
+            start(copy(slot, from_chip(d, core), part, other))
+            source = from_chip(d, 1 - core)
+            at(transit("core", amount, 1, 300e3), lambda: near(slot, source, part))
+
+        def far(d):
+            copy(d, from_chip(d, core), whole, from_chip(d, core)).wait_recv()
+            half, onward, slot, hop = (0, 1, 2, 1) if d == 1 else (1, 3, 4, -1)
+            start(copy(slot, from_chip(d, core), halves[half], from_chip(-onward, core)))
+            at(transit(("x", hop), size / 2), lambda: farther(slot, half))
+            to_core(4 + d, d, whole, size)
+
+        def farther(slot, half):
+            copy(slot, from_chip(2, core), halves[half], other).wait_recv()
+            to_core(4 + slot, 2, halves[half], size / 2)
+
+        for d, hop in ((1, 1), (3, -1)):
+            start(copy(d, t, whole, step_to(chip, d, CHIPS) * 2 + core))
+            at(transit(("x", hop), size), lambda d=d: far(d))
+        start(copy(0, t, whole, other))
+        at(transit("core", size, 1, 300e3), lambda: near(0, other, whole))
+
     quarter = SIDE // 2
-    deep1, deep2 = ws1.shape[2] // 2, wc2.shape[2] // 2
-    piece = ws1.shape[2] * ws1.shape[3] * 2
-
-    def rows_of(half, deep):
-        return pl.ds(half * deep, deep)
-
-    def after(*names):
-        for name in names:
-            loads[name].wait()
-
-    def direct(number):
-        return (
-            lambda d: ring_send.at[number, d],
-            lambda d: ring_recv.at[number, d],
-        )
+    unit1 = ws1.shape[2] * part_width * 2
 
     def both(fn):
         return when_all(2, fn)
 
-    state_in = ring(
-        0, "z", lambda i, h: ws1.at[i, pl.ds(h * quarter, quarter)], 4 * piece,
-        lambda: at(clock[0], recur, 1.8), lambda: go_sv(),
+    s1_big = ring(
+        0, "z", lambda i, h: ws1.at[i, pl.ds(h * quarter, quarter)], 4 * unit1,
+        lambda: (s1_own(), s1_far()), lambda: go_s2(),
     )
-    sv_big = ring(
-        1, "z", lambda i, h: ws2.at[0, i, pl.ds(h * quarter, quarter)], 4 * piece,
-        lambda: state_ready(), lambda: go_sg(),
+    s2_big = ring(
+        1, "z", lambda i, h: ws2.at[i, pl.ds(h * quarter, quarter)], 8 * unit1,
+        lambda: (state_own(), state_far()),
     )
-    sg_big = ring(
-        2, "z", lambda i, h: ws2.at[1, i, pl.ds(h * quarter, quarter)], 4 * piece,
-        lambda: state_ready(),
+    c1_big = ring(
+        2, "y", lambda i, h: wc1.at[pl.ds(h * quarter, quarter), i], 8 * unit1,
+        lambda: (c1_own(), c1_far()), lambda: go_c2(),
     )
-    go_sv, go_sg = both(sv_big), both(sg_big)
-    sg_small = ring(
-        3, "y", lambda i, h: ws2.at[1, z, i, rows_of(h, deep2)], piece / 2, lambda: go_sg()
+    c2_big = ring(
+        3, "y", lambda i, h: wc2.at[pl.ds(h * quarter, quarter), i], 4 * unit1,
+        lambda: (conv_own(), conv_far()),
     )
-    sv_small = ring(
-        4, "y", lambda i, h: ws2.at[0, z, i, rows_of(h, deep2)], piece / 2,
-        lambda: (go_sv(), sg_small()),
-    )
-    conv_in = ring(
-        5, "y", lambda i, h: wc1.at[0, pl.ds(h * quarter, quarter), i], 4 * piece,
-        lambda: gate_ready(), lambda: go_cg(),
-    )
-    cg_big = ring(
-        6, "y", lambda i, h: wc1.at[1, pl.ds(h * quarter, quarter), i], 4 * piece,
-        lambda: gate_ready(), lambda: go_cp(),
-    )
-    cp_big = ring(
-        7, "y", lambda i, h: wc2.at[pl.ds(h * quarter, quarter), i], 4 * piece,
-        lambda: conv_ready(),
-    )
-    go_cg, go_cp = both(cg_big), both(cp_big)
-    cp_small = ring(
-        8, "z", lambda i, h: wc2.at[i, y, rows_of(h, deep2)], piece / 2, lambda: go_cp()
-    )
-    cg_small = ring(
-        9, "z", lambda i, h: wc1.at[1, i, y, rows_of(h, deep1)], piece / 2,
-        lambda: (go_cg(), cp_small()),
-    )
-    sf_small = spread_out(direct(10), "y", lambda i: ws1.at[z, i], piece, state_in)
-    cv_small = spread_out(direct(11), "z", lambda i: wc1.at[0, i, y], piece, conv_in)
+    go_s2, go_c2 = both(s2_big), both(c2_big)
+    s1_small = deal(4, "y", stage_s1, lambda i: ws1.at[z, i], unit1, s1_big)
+    c1_small = deal(5, "z", stage_c1, lambda i: wc1.at[i, y], 2 * unit1, c1_big)
+    s2_small = deal(6, "y", stage_s2, lambda i: ws2.at[z, i], 2 * unit1, lambda: go_s2())
+    c2_small = deal(7, "z", stage_c2, lambda i: wc2.at[i, y], unit1, lambda: go_c2())
 
     def begin():
-        after("ws1")
-        sf_small()
-        after("wc1v")
-        cv_small()
-        after("wc1g")
-        cg_small()
+        after("s1")
+        s1_small()
+        after("c1")
+        c1_small()
+
+    def begin_second():
+        after("s2", "c2")
+        c2_small()
+        s2_small()
 
     at(0.0, begin)
-    at(5.0, lambda: (after("ws2v", "ws2g", "wc2"), sv_small()))
-
-    def normalise():
-        loads["raw"].wait()
+    at(10.0, begin_second)
+
+    step = normed.shape[3]
+
+    def measure():
+        after("raw", "small")
         def body(i, carry):
             part = pl.ds(pl.multiple_of(i * 16, 16), 16)
             value = raw[part, :].astype(F32)
-            scale = lax.rsqrt(jnp.mean(value * value, axis=1, keepdims=True) + 1e-6)
-            normed[part, :] = (value * scale * norm_gain[...]).astype(BF)
+            mean = jnp.mean(value * value, axis=1, keepdims=True)
+            scale[part, :] = jnp.broadcast_to(lax.rsqrt(mean + 1e-6), (16, 128))
             return carry
         lax.fori_loop(0, length // 16, body, 0)
+        normalise(t)
+        for i, axis in ((1, "y"), (2, "z")):
+            hand_over(
+                i, axis, normed.at[0, t], normed.at[i, t], normed.at[i, t], length * step * 2,
+                lambda i=i: share(
+                    i, lambda c: normed.at[i, c], length, length * step * 2,
+                    (lambda: s1_far()) if i == 1 else (lambda: c1_far()),
+                ),
+            )
+
+    def normalise(c):
+        lanes = lanes_from(c, step)
+        value = raw[:, lanes].astype(F32)
+        normed[0, c] = (value * scale[:, 0:1] * norm_gain[:, lanes]).astype(BF)
+
+    def normalise_all():
+        def body(c, carry):
+            pl.when(c != t)(lambda: normalise(c))
+            return carry
+        lax.fori_loop(0, 2 * CHIPS, body, 0)
 
     def spread():
         return ((iota((size, flat), 1) & (size - 1)) == iota((size, flat), 0)).astype(F32)
@@ -335,17 +453,40 @@
         fill(output_real, 1.0, emit, slice(0, flat))
         fill(output_imag, -1.0, emit, slice(flat, 2 * flat))
 
-    at(8.0, normalise, 1.8)
-    at(9.0, tables, 1.4)
-    at(11.0, matrices, 1.0)
+    at(0.5, measure, 1.0)
+    at(6.0, normalise_all, 1.5)
+    at(8.0, tables, 1.4)
+    at(9.0, matrices, 1.0)
 
     chunk = 256
 
+    def project_in(i, weights):
+        count = weights.shape[3]
+        total = None
+        for c in range(2 * CHIPS):
+            term = jnp.dot(normed[i, c], weights[c].reshape(step, count), preferred_element_type=F32)
+            total = term if total is None else total + term
+        return total
+
+    def feed_own():
+        feed_half[odd["y"]] = project_in(0, ws1).astype(BF)
+        recur_ready()
+
+    def feed_far():
+        feed_back[...] = project_in(1, ws1).astype(BF)
+        hand_over(
+            3, "y", feed_back, feed_half.at[odd["y"]], feed_half.at[1 - odd["y"]],
+            length * part_width * 2, lambda: recur_ready(),
+        )
+
+    s1_own = when_all(1, lambda: at(clock[0], feed_own, 0.6))
+    s1_far = both(lambda: at(clock[0], feed_far, 0.6))
+    recur_ready = both(lambda: at(clock[0], recur, 1.4))
+
     def recur():
-        drive = jnp.dot(
-            normed[...], ws1[...].reshape(normed.shape[1], width), preferred_element_type=F32
-        ).astype(BF)
-        feed[...] = drive
+        feed[:, 0:part_width] = feed_half[0]
+        feed[:, part_width:width] = feed_half[1]
+        drive = feed[...]
         for j in range(flat // chunk):
             part = slice(j * chunk, (j + 1) * chunk)
             shift = slice(flat + j * chunk, flat + (j + 1) * chunk)
@@ -405,6 +546,7 @@
             sum_i = next_i + totals[zz, :, flat:2 * flat]
         final_state[0] = as_table(sum_r)
         final_state[1] = as_table(sum_i)
+        load("final", final_state, final_out)
         lead_r, lead_i = rotate(rows[8:9, :], rows[9:10, :], start_r, start_i)
         entry_r, entry_i = lead_r + rows[6:7, :], lead_i + rows[7:8, :]
         for j in range(flat // chunk):
@@ -418,69 +560,60 @@
             states[:, shift] = state_i.astype(BF)
         answer = lax.dot_general(states[...], emit[...], NT, preferred_element_type=F32)
         answer = answer + skip_gain[...] * feed[...].astype(F32)
-        act_all[t] = jax.nn.gelu(answer).astype(BF)
-        share(0, act_all, lambda: state_ready())
-
-    other = t + 1 - 2 * core
-
-    def share(number, blocks, done):
-        finished = when_all(4, done)
-        size = length * width * 2
-
-        def copy(slot, source, to):
-            return remote(
-                blocks.at[source], blocks.at[source], tp_send.at[number, slot],
-                tp_recv.at[number, slot], device(z, y, to),
+        act_all[0, t] = jax.nn.gelu(answer).astype(BF)
+        exchange(3, "y", act_all, lambda: state_own(), lambda: state_far())
+
+    def exchange(number, axis, blocks, own, far):
+        amount = length * width * 2
+        hand_over(
+            number + 1, axis, blocks.at[0, t], blocks.at[1, t], blocks.at[1, t], amount,
+            lambda: share(number + 1, lambda c: blocks.at[1, c], length, amount, far),
+        )
+        share(number, lambda c: blocks.at[0, c], length, amount, own)
+
+    edge = halo.shape[1]
+    kernel_size = conv_taps.shape[0]
+
+    def gate(i):
+        pair = project_in(i, wc1)
+        return (pair[:, 0:part_width] * jax.nn.sigmoid(pair[:, part_width:width])).astype(BF)
+
+    def gate_own():
+        gated_half[odd["z"]] = gate(0)
+        gate_ready()
+
+    def gate_far():
+        gated_back[...] = gate(2)
+        hand_over(
+            5, "z", gated_back, gated_half.at[odd["z"]], gated_half.at[1 - odd["z"]],
+            length * part_width * 2, lambda: gate_ready(),
+        )
+
+    c1_own = when_all(1, lambda: at(clock[0], gate_own, 0.7))
+    c1_far = both(lambda: at(clock[0], gate_far, 0.7))
+    gate_ready = both(lambda: at(clock[0], pass_edge, 0.1))
+    last = pl.ds(length - edge, edge)
+
+    def pass_edge():
+        start(
+            remote(
+                gated_half.at[:, last], halo, halo_sem.at[0], halo_sem.at[1],
+                {"sp": following, "tp": t},
             )
-
-        def start(moving):
-            moving.start()
-            sent.append(moving)
-
-        def near(d):
-            source = other if d == 0 else step_to(chip, -d, CHIPS) * 2 + 1 - core
-            copy(3 + d if d else 0, source, other).wait_recv()
-            finished()
-
-        def far(d):
-            source = step_to(chip, -d, CHIPS) * 2 + core
-            copy(d, source, source).wait_recv()
-            start(copy(3 + d, source, other))
-            at(transit("core", size, 1, 300e3), lambda: near(d))
-
-        for d in (2, 1, 3):
-            start(copy(d, t, step_to(chip, d, CHIPS) * 2 + core))
-            time = transit(("x", -1 if d == 3 else 1), size, 2 if d == 2 else 1)
-            at(time, lambda d=d: far(d))
-        start(copy(0, t, other))
-        at(transit("core", size, 1, 300e3), lambda: near(0))
-
-    edge = halo.shape[0]
-    kernel_size = conv_taps.shape[0]
-
-    def gate():
-        value_in = jnp.dot(
-            normed[...], wc1[0].reshape(normed.shape[1], width), preferred_element_type=F32
-        )
-        gate_in = jnp.dot(
-            normed[...], wc1[1].reshape(normed.shape[1], width), preferred_element_type=F32
-        )
-        gated[...] = (value_in * jax.nn.sigmoid(gate_in)).astype(BF)
-        moving = remote(
-            gated.at[pl.ds(length - edge, edge)], halo, halo_sem.at[0], halo_sem.at[1],
-            {"sp": following, "tp": t},
-        )
-        moving.start()
-        sent.append(moving)
+        )
         at(transit(("y", 1), edge * width * 2), convolve, 0.7)
-        padded[edge:edge + length, :] = gated[...].astype(F32)
+        for half in (0, 1):
+            lanes = slice(half * part_width, (half + 1) * part_width)
+            padded[edge:edge + length, lanes] = gated_half[half].astype(F32)
 
     def convolve():
         remote(
-            gated.at[pl.ds(length - edge, edge)], halo, halo_sem.at[0], halo_sem.at[1],
+            gated_half.at[:, last], halo, halo_sem.at[0], halo_sem.at[1],
             {"sp": preceding, "tp": t},
         ).wait_recv()
-        padded[0:edge, :] = jnp.where(seq > 0, halo[...].astype(F32), 0.0)
+        for half in (0, 1):
+            lanes = slice(half * part_width, (half + 1) * part_width)
+            padded[0:edge, lanes] = jnp.where(seq > 0, halo[half].astype(F32), 0.0)
         lag = edge - (kernel_size - 1)
         for lane in range(width // 128):
             lanes = slice(lane * 128, (lane + 1) * 128)
@@ -497,14 +630,17 @@
                     answer = answer + shifted[b, b:b + length, :]
                 else:
                     answer = answer + part
-            conv_all[t, :, lanes] = answer.astype(BF)
-        share(1, conv_all, lambda: at(clock[0], channel_norm, 2.0))
-
-    def channel_norm():
+            conv_all[0, t, :, lanes] = answer.astype(BF)
+        exchange(
+            6, "z", conv_all, lambda: at(clock[0], lambda: channel_norm(0), 2.5),
+            lambda: at(clock[0], lambda: channel_norm(1), 2.5),
+        )
+
+    def channel_norm(which):
         count = 2 * CHIPS * width
         def body(i, carry):
             part = pl.ds(pl.multiple_of(i * 16, 16), 16)
-            pieces = [conv_all[c, part, :].astype(F32) for c in range(2 * CHIPS)]
+            pieces = [conv_all[which, c, part, :].astype(F32) for c in range(2 * CHIPS)]
             total = pieces[0]
             for piece in pieces[1:]:
                 total = total + piece
@@ -517,43 +653,68 @@
             for c, piece in enumerate(pieces):
                 lanes = slice(c * width, (c + 1) * width)
                 value = piece * scale * chan_gain[:, lanes] + chan_shift[:, lanes]
-                conv_act[c, part, :] = jax.nn.silu(value).astype(BF)
+                conv_act[which, c, part, :] = jax.nn.silu(value).astype(BF)
             return carry
         lax.fori_loop(0, length // 16, body, 0)
-        conv_ready()
-
-    columns = out.shape[1]
-
-    def project(blocks, weights, lanes):
+        (conv_far if which else conv_own)()
+
+    def project(blocks, i, weights):
+        count = weights.shape[3]
         total = None
         for c in range(2 * CHIPS):
             term = jnp.dot(
-                blocks[c], weights[c].reshape(width, columns)[:, lanes], preferred_element_type=F32
+                blocks[i, c], weights[c].reshape(width, count), preferred_element_type=F32
             )
             total = term if total is None else total + term
         return total
 
-    def state_out():
-        for n in range(columns // 256):
-            lanes = slice(n * 256, (n + 1) * 256)
-            mixed[:, lanes] = project(act_all, ws2.at[0], lanes) * jax.nn.sigmoid(
-                project(act_all, ws2.at[1], lanes)
-            )
-        conv_ready()
-
-    def conv_out():
-        for n in range(columns // 256):
-            lanes = slice(n * 256, (n + 1) * 256)
-            result[:, lanes] = (mixed[:, lanes] + project(conv_act, wc2, lanes)).astype(BF)
-        moving = pltpu.make_async_copy(result, out, load_sem.at[7])
-        moving.start()
-        for copy in sent:
-            copy.wait_send()
-        moving.wait()
-
-    state_ready = when_all(3, lambda: at(clock[0], state_out, 1.4))
-    gate_ready = both(lambda: at(clock[0], gate, 1.0))
-    conv_ready = when_all(3, lambda: at(clock[0], conv_out, 1.4))
+    def state_out(i):
+        pair = project(act_all, i, ws2)
+        return pair[:, 0:part_columns] * jax.nn.sigmoid(pair[:, part_columns:columns])
+
+    def state_out_own():
+        state_half[odd["y"]] = state_out(0)
+        finish_ready()
+
+    def state_out_far():
+        state_back[...] = state_out(1).astype(BF)
+        hand_over(
+            6, "y", state_back, state_got, state_got, length * part_columns * 2, state_returned
+        )
+
+    def state_returned():
+        state_half[1 - odd["y"]] = state_got[...].astype(F32)
+        finish_ready()
+
+    def conv_out_own():
+        conv_half[odd["z"]] = project(conv_act, 0, wc2)
+        finish_ready()
+
+    def conv_out_far():
+        conv_back[...] = project(conv_act, 1, wc2).astype(BF)
+        hand_over(8, "z", conv_back, conv_got, conv_got, length * part_columns * 2, conv_returned)
+
+    def conv_returned():
+        conv_half[1 - odd["z"]] = conv_got[...].astype(F32)
+        finish_ready()
+
+    state_own = both(lambda: at(clock[0], state_out_own, 0.8))
+    state_far = both(lambda: at(clock[0], state_out_far, 0.8))
+    conv_own = both(lambda: at(clock[0], conv_out_own, 0.6))
+    conv_far = both(lambda: at(clock[0], conv_out_far, 0.6))
+    finish_ready = when_all(4, lambda: at(clock[0], finish, 0.5))
+
+    def finish():
+        for half in (0, 1):
+            lanes = slice(half * part_columns, (half + 1) * part_columns)
+            result[:, lanes] = (state_half[half] + conv_half[half]).astype(BF)
+        load("out", result, out)
+        drain(1e9)
+        after("final", "out")
+
+    at(35.0, lambda: drain(25.0))
+    at(48.0, lambda: drain(38.0))
+    at(57.0, lambda: drain(50.0))
     run()
 
 
@@ -572,34 +733,36 @@
         tokens, norm_gain.reshape(1, -1), conv_value, conv_gate, state_feed, conv_taps,
         chan_gain.reshape(1, -1), chan_shift.reshape(1, -1), conv_project, decay_rate, frequency,
         jnp.swapaxes(input_real, 1, 2), jnp.swapaxes(input_imag, 1, 2), output_real, output_imag,
-        skip_gain.reshape(1, -1), state_value,
-        state_gate, initial_state,
+        skip_gain.reshape(1, -1), state_value, state_gate, initial_state,
     )
-    large = {0, 2, 3, 4, 8, 16, 17}
     anywhere = pl.BlockSpec(memory_space=pl.ANY)
-    held = pl.BlockSpec(memory_space=pltpu.VMEM)
     vmem = pltpu.VMEM
     dma = pltpu.SemaphoreType.DMA
+    many = 2 * CHIPS
     return pl.pallas_call(
         kernel,
         out_shape=(
             jax.ShapeDtypeStruct((length, columns), BF),
             jax.ShapeDtypeStruct(initial_state.shape, F32),
         ),
-        in_specs=[anywhere if i in large else held for i in range(len(args))],
-        out_specs=(anywhere, held),
+        in_specs=[anywhere] * len(args),
+        out_specs=(anywhere, anywhere),
         scratch_shapes=[
+            *(vmem(args[i].shape, args[i].dtype) for i in SMALL),
+            vmem((SIDE, SIDE, deep1, width // 2), BF),
             vmem((SIDE, SIDE, deep1, width), BF),
-            vmem((2, SIDE, SIDE, deep1, width), BF),
-            vmem((2, SIDE, SIDE, deep2, columns), BF),
             vmem((SIDE, SIDE, deep2, columns), BF),
+            vmem((SIDE, SIDE, deep2, columns // 2), BF),
+            vmem((2, deep1, width // 2), BF),
+            vmem((2, deep1, width), BF),
+            vmem((2, deep2, columns), BF),
+            vmem((2, deep2, columns // 2), BF),
             vmem((length, features), BF),
-            vmem((length, features), BF),
+            vmem((length, 128), F32),
+            vmem((3, many, length, features // many), BF),
             vmem((length, columns), BF),
-            vmem((length, flat), F32),
-            vmem((length, flat), F32),
-            vmem((length, flat), F32),
-            vmem((length, flat), F32),
+            vmem(initial_state.shape, F32),
+            *(vmem((length, flat), F32) for _ in range(4)),
             vmem((width, flat), BF),
             vmem((width, flat), BF),
             vmem((width, 2 * flat), BF),
@@ -610,25 +773,36 @@
             vmem((16, flat), F32),
             vmem((SIDE, 1, 2 * flat), F32),
             vmem((SIDE, 1, 2 * flat), F32),
-            vmem((length, width), BF),
-            vmem((edge, width), BF),
+            vmem((2, length, width // 2), BF),
+            vmem((length, width // 2), BF),
+            vmem((2, length, width // 2), BF),
+            vmem((length, width // 2), BF),
+            vmem((2, edge, width // 2), BF),
             vmem((edge + length, width), F32),
             vmem((8, length + 8, 128), F32),
-            vmem((2 * CHIPS, length, width), BF),
-            vmem((2 * CHIPS, length, width), BF),
-            vmem((2 * CHIPS, length, width), BF),
-            vmem((length, columns), F32),
-            dma((8,)),
-            dma((12, len(SLOTS))),
-            dma((12, len(SLOTS))),
+            *(vmem((2, many, length, width), BF) for _ in range(3)),
+            *(
+                vmem(shape, held)
+                for _ in range(2)
+                for shape, held in (
+                    ((2, length, columns // 2), F32),
+                    ((length, columns // 2), BF),
+                    ((length, columns // 2), BF),
+                )
+            ),
+            dma((40,)),
+            dma((8, len(SLOTS))),
+            dma((8, len(SLOTS))),
             dma((2, SIDE - 1)),
             dma((2, SIDE - 1)),
             dma((2,)),
-            dma((2, 7)),
-            dma((2, 7)),
+            dma((8, 9)),
+            dma((8, 9)),
+            dma((9,)),
+            dma((9,)),
         ],
         compiler_params=pltpu.CompilerParams(
-            collective_id=0, has_side_effects=True, vmem_limit_bytes=60 * 1024 * 1024
+            collective_id=0, has_side_effects=True, vmem_limit_bytes=62 * 1024 * 1024
         ),
         name="mixer",
     )(*args)

time: 113 us -> 101 us (0.89)
  Pallas kernels: 109 us -> 96.7 us
    pallas_call x1, Pallas kernels: 109 us -> 96.7 us  [local(): pl.pallas_call(kernel, out_shape=(jax.ShapeDtypeStruct((length, columns),...]
where the time goes in v3:
time: 101 us; the launch traced here: 100 us
  Pallas kernels  96.7 us (96%)
  local copies, waits for them, and re-layouts  2.94 us (3%)
    pallas_call x1, Pallas kernels, local(): pl.pallas_call(kernel, out_shape=(jax.ShapeDtypeStruct((length, columns),...  96.7 us
    unnamed x2, local copies, waits for them, and re-layouts  2.94 us

profile of v3, /device:TPU:1, one launch (start us, length us, event | category | flops | bytes accessed | tf_op | source)
XLA Modules:
  0.0 100.3 jit_solution(7173956598557100102)
XLA Ops:
  0.6 96.7 %mixer.1 = (bf16[192,512]{1,0:T(8,128)(2,1)}, f32[2,16,64]{2,1,0:T(8,128)}) custom-call(bf16[192,4096]{1,0:T(8,128)(2,1)} %refs_0_.1, f32[1,4096]{1,0:T(1,128)} %bitcast.8, bf16[64,256]{1,0:T(8,128)(2,1)} %refs_2_.1, bf16[64,256]{1,0:T(8,128)(2,1)} %refs_3_.1, bf16[64,256]{1,0:T(8,128)(2,1)} %refs_4_.1, f32[31,256]{1,0:T(8,128)} %refs_5_.1, ...), custom_call_target="tpu_custom_call" | custom-call | tf_op jit(solution)/shard_map/mixer/pallas_call | solution.py:742
  97.3 1.6 %copy.23 = bf16[192,512]{1,0:T(8,128)(2,1)} copy(bf16[192,512]{1,0:T(8,128)(2,1)} %get-tuple-element.4) | data formatting | bytes 393216
  99.0 1.3 %copy.24 = f32[2,16,64]{2,1,0:T(8,128)} copy(f32[2,16,64]{2,1,0:T(8,128)} %get-tuple-element.5) | data formatting | bytes 16384

commit v4 on v3

--- a/solution.py
+++ b/solution.py
@@ -11,6 +11,9 @@
 HIGHEST = lax.Precision.HIGHEST
 MESH = pl.DeviceIdType.MESH
 SIDE = 8
+WINDOW = (2, 2, 9, 2)
+WHEN = (16.0, 14.0, 12.0)
+CLASSES = ((0,), (1, 7, 2, 6), (3, 5, 4))
 CHIPS = 4
 NT = (((1,), (1,)), ((), ()))
 
@@ -19,13 +22,8 @@
     return SIDE // 2 if (direction > 0) == (half == 0) else SIDE // 2 - 1
 
 
-SLOTS = [
-    (direction, half, k)
-    for direction in (1, -1)
-    for half in (0, 1)
-    for k in range(hops(direction, half))
-]
-SLOT_OF = {slot: at for at, slot in enumerate(SLOTS)}
+def slot_of(direction, half, k):
+    return k if direction > 0 else hops(1, half) + k
 
 
 def rotate(first_real, first_imag, second_real, second_imag):
@@ -56,7 +54,7 @@
         shifted, conv_all, act_all, conv_act, state_half, state_back, state_got, conv_half, conv_back,
         conv_got,
         load_sem, ring_send, ring_recv, scan_send, scan_recv, halo_sem, tp_send, tp_recv, pair_send,
-        pair_recv,
+        pair_recv, deal_send, deal_recv,
     ) = refs[21 + len(SMALL):]
     seq = lax.axis_index("sp")
     t = lax.axis_index("tp")
@@ -101,6 +99,8 @@
         moving.start()
         sent.append((clock[0], moving))
 
+    closing = []
+
     def drain(before):
         kept = []
         for time, moving in sent:
@@ -127,15 +127,20 @@
     loads, counted = {}, []
 
     def load(name, src, dst):
-        moving = pltpu.make_async_copy(src, dst, load_sem.at[len(counted)])
+        if name not in counted:
+            counted.append(name)
+        moving = pltpu.make_async_copy(src, dst, load_sem.at[counted.index(name)])
         moving.start()
-        counted.append(name)
-        loads.setdefault(name, []).append(moving)
-
-    def after(*names):
-        for name in names:
-            for moving in loads.pop(name, []):
-                moving.wait()
+        loads[name] = moving
+
+    def bytes_of(ref, sem):
+        pltpu.make_async_copy(ref, ref, sem).wait()
+
+    def after(name, three=None):
+        if three is None:
+            loads[name].wait()
+        else:
+            bytes_of(three, load_sem.at[counted.index(name)])
 
     here = {"z": z, "y": y}
     odd = {"z": z % 2, "y": y % 2}
@@ -159,7 +164,7 @@
     staged("c1", "z", (conv_value, conv_gate), stage_c1, wc1.at[z, y], part_width)
     load("raw", tokens, raw)
     for i, place in enumerate(SMALL):
-        load("small", refs[place], small[i])
+        load(place, refs[place], small[i])
     (
         norm_gain, conv_taps, chan_gain, chan_shift, decay_rate, frequency, input_real, input_imag,
         output_real, output_imag, skip_gain, initial_state,
@@ -186,79 +191,104 @@
         moved = step_to(here[axis], by, SIDE)
         return device(moved, y, t) if axis == "z" else device(z, moved, t)
 
-    def ring(number, axis, block, size, done, nearly=None):
+    def spread_out(number, axis, blocks, size, done):
         position = here[axis]
-        finished = when_all(len(SLOTS), done)
-        passed = when_all(len(SLOTS) - 4, nearly or (lambda: None))
-
-        def copy(direction, half, k, source):
-            slot = SLOT_OF[(direction, half, k)]
+        all_others = blocks.at[pl.ds(0, SIDE - 1)]
+        latest = 0.0
+        for d in (4, 3, 5, 2, 6, 1, 7):
+            remote(
+                blocks.at[position], blocks.at[position], scan_send.at[number],
+                scan_recv.at[number], beside(axis, d),
+            ).start()
+            direction, count = (1, d) if d <= SIDE // 2 else (-1, SIDE - d)
+            latest = max(latest, transit((axis, direction), size, count))
+
+        def arrived():
+            bytes_of(all_others, scan_recv.at[number])
+            done()
+        at(latest, arrived)
+        closing.append(lambda: bytes_of(all_others, scan_send.at[number]))
+
+    def trains(number, axis, across, stage, block, several, size, window, done, nearly=None):
+        position, lane = here[axis], here[across]
+        members = [
+            (which, direction, k)
+            for which in range(len(CLASSES)) for direction in (1, -1) for k in range(SIDE // 2)
+            if any(k < hops(direction, d % 2) for d in CLASSES[which])
+        ]
+        finished = when_all(len(members), done)
+        passed = when_all(len(CLASSES), nearly or (lambda: None))
+        ready, active = [], [0]
+        left = [len(c) * (SIDE - 1) for c in CLASSES]
+
+        def dealt(d, source, to):
+            half = odd[across] if d % 2 == 0 else 1 - odd[across]
             return remote(
-                block(source, half), block(source, half),
-                ring_send.at[number, slot], ring_recv.at[number, slot], beside(axis, direction),
+                stage.at[half], block(position, source), deal_send.at[number],
+                deal_recv.at[number, int(d in CLASSES[-1])], to,
             )
 
-        def send(direction, half, k):
-            moving = copy(direction, half, k, step_to(position, -direction * k, SIDE))
-            start(moving)
-            time = transit((axis, direction), size)
-            at(time, lambda: arrived(direction, half, k))
-
-        def arrived(direction, half, k):
-            source = step_to(position, -direction * (k + 1), SIDE)
-            copy(direction, half, k, source).wait_recv()
-            if k + 1 < hops(direction, half):
-                send(direction, half, k + 1)
+        def slot(which, direction, k):
+            return members.index((which, direction, k))
+
+        def copy(which, d, direction, k, source):
+            held = block(source, step_to(lane, -d, SIDE))
+            return remote(
+                held, held, ring_send.at[number], ring_recv.at[number, slot(which, direction, k)],
+                beside(axis, direction),
+            )
+
+        def send(which, direction, k):
+            time = 0.0
+            for d in CLASSES[which]:
+                if k < hops(direction, d % 2):
+                    copy(which, d, direction, k, step_to(position, -direction * k, SIDE)).start()
+                    time = transit((axis, direction), size)
+                    left[which] -= 1
+            at(time, lambda: arrived(which, direction, k))
+            if left[which] == 0:
+                active[0] -= 1
                 passed()
+
+        def arrived(which, direction, k):
+            count = sum(k < hops(direction, d % 2) for d in CLASSES[which])
+            bytes_of(several(count), ring_recv.at[number, slot(which, direction, k)])
+            if any(k + 1 < hops(direction, d % 2) for d in CLASSES[which]):
+                send(which, direction, k + 1)
+                inject()
             finished()
 
-        def first():
-            for half in (0, 1):
+        def inject():
+            while ready and active[0] < window[0]:
+                which = ready.pop(0)
+                active[0] += 1
                 for direction in (1, -1):
-                    send(direction, half, 0)
-        return first
-
-    def spread_out(sems, axis, block, size, done):
-        position = here[axis]
-        finished = when_all(SIDE - 1, done)
-
-        def copy(d, source, to):
-            return remote(block(source), block(source), sems[0](d), sems[1](d), to)
-
-        def arrived(d):
-            copy(d, step_to(position, -d, SIDE), beside(axis, -d)).wait_recv()
-            finished()
-
-        def first():
-            for d in (4, 3, 5, 2, 6, 1, 7):
-                moving = copy(d, position, beside(axis, d))
-                start(moving)
-                direction, count = (1, d) if d <= SIDE // 2 else (-1, SIDE - d)
-                time = transit((axis, direction), size, count)
-                at(time, lambda d=d: arrived(d))
-        return first
-
-    def deal(number, axis, stage, block, size, done):
-        position = here[axis]
-        finished = when_all(SIDE - 1, done)
-
-        def copy(d, source, to):
-            half = odd[axis] if d % 2 == 0 else 1 - odd[axis]
-            return remote(
-                stage.at[half], block(source), ring_send.at[number, d], ring_recv.at[number, d], to
-            )
-
-        def arrived(d):
-            copy(d, step_to(position, -d, SIDE), beside(axis, -d)).wait_recv()
-            finished()
-
-        def first():
-            for d in (4, 3, 5, 2, 6, 1, 7):
-                start(copy(d, position, beside(axis, d)))
-                direction, count = (1, d) if d <= SIDE // 2 else (-1, SIDE - d)
-                time = transit((axis, direction), size, count)
-                at(time, lambda d=d: arrived(d))
-        return first
+                    send(which, direction, 0)
+
+        def received(which):
+            count = len(CLASSES[2]) if which else SIDE - 1 - len(CLASSES[2])
+            bytes_of(several(count), deal_recv.at[number, which])
+            ready.extend([2] if which else list(range(1, len(CLASSES) - 1)))
+            inject()
+
+        def deal():
+            for which, members_of in enumerate(((1, 7, 2, 6), CLASSES[-1])):
+                time = 0.0
+                for d in members_of:
+                    dealt(d, lane, beside(across, d)).start()
+                    direction, count = (1, d) if d <= SIDE // 2 else (-1, SIDE - d)
+                    time = max(time, transit((across, direction), size, count))
+                at(time, lambda which=which: received(which))
+            ready.insert(0, 0)
+            inject()
+
+        def go(amount):
+            window[0] = amount
+            inject()
+
+        closing.append(lambda: bytes_of(block(pl.ds(0, SIDE - 1), pl.ds(0, SIDE)), ring_send.at[number]))
+        closing.append(lambda: bytes_of(several(SIDE - 1), deal_send.at[number]))
+        return deal, go
 
     def mate(axis):
         other_one = here[axis] + 1 - 2 * odd[axis]
@@ -276,107 +306,109 @@
     other = t + 1 - 2 * core
 
     def share(number, block, tall, size, done):
-        finished = when_all(5, done)
         halves = (pl.ds(0, tall // 2), pl.ds(tall // 2, tall // 2))
         whole = pl.ds(0, tall)
+        near_sem = tp_recv.at[number, 0]
 
         def copy(slot, source, part, to):
             return remote(
-                block(source).at[part], block(source).at[part], tp_send.at[number, slot],
+                block(source).at[part], block(source).at[part], tp_send.at[number],
                 tp_recv.at[number, slot], device(z, y, to),
             )
 
         def from_chip(d, which):
             return step_to(chip, -d, CHIPS) * 2 + which
 
-        def near(slot, source, part):
-            copy(slot, source, part, other).wait_recv()
-            finished()
-
-        def to_core(slot, d, part, amount):
-            start(copy(slot, from_chip(d, core), part, other))
-            source = from_chip(d, 1 - core)
-            at(transit("core", amount, 1, 300e3), lambda: near(slot, source, part))
+        def near():
+            bytes_of(block(pl.ds(0, CHIPS)), near_sem)
+            done()
+
+        latest = [0.0]
+        all_near = when_all(5, lambda: at(latest[0], near))
+
+        def to_core(source, part, amount):
+            copy(0, source, part, other).start()
+            latest[0] = max(latest[0], transit("core", amount, 1, 300e3))
+            all_near()
 
         def far(d):
             copy(d, from_chip(d, core), whole, from_chip(d, core)).wait_recv()
             half, onward, slot, hop = (0, 1, 2, 1) if d == 1 else (1, 3, 4, -1)
-            start(copy(slot, from_chip(d, core), halves[half], from_chip(-onward, core)))
+            copy(slot, from_chip(d, core), halves[half], from_chip(-onward, core)).start()
             at(transit(("x", hop), size / 2), lambda: farther(slot, half))
-            to_core(4 + d, d, whole, size)
+            to_core(from_chip(d, core), whole, size)
 
         def farther(slot, half):
             copy(slot, from_chip(2, core), halves[half], other).wait_recv()
-            to_core(4 + slot, 2, halves[half], size / 2)
+            to_core(from_chip(2, core), halves[half], size / 2)
 
         for d, hop in ((1, 1), (3, -1)):
-            start(copy(d, t, whole, step_to(chip, d, CHIPS) * 2 + core))
+            copy(d, t, whole, step_to(chip, d, CHIPS) * 2 + core).start()
             at(transit(("x", hop), size), lambda d=d: far(d))
-        start(copy(0, t, whole, other))
-        at(transit("core", size, 1, 300e3), lambda: near(0, other, whole))
-
-    quarter = SIDE // 2
+        to_core(t, whole, size)
+        closing.append(lambda: bytes_of(block(pl.ds(0, 2 * CHIPS - 1)), tp_send.at[number]))
+
     unit1 = ws1.shape[2] * part_width * 2
 
     def both(fn):
         return when_all(2, fn)
 
-    s1_big = ring(
-        0, "z", lambda i, h: ws1.at[i, pl.ds(h * quarter, quarter)], 4 * unit1,
-        lambda: (s1_own(), s1_far()), lambda: go_s2(),
+    deal_s1, _ = trains(
+        0, "z", "y", stage_s1, lambda r, p: ws1.at[r, p], lambda n: ws1.at[0, pl.ds(0, n)], unit1, [WINDOW[0]],
+        lambda: (s1_far(), s1_own()), lambda: go_s2(WINDOW[1]),
     )
-    s2_big = ring(
-        1, "z", lambda i, h: ws2.at[i, pl.ds(h * quarter, quarter)], 8 * unit1,
+    deal_c1, _ = trains(
+        1, "y", "z", stage_c1, lambda r, p: wc1.at[p, r], lambda n: wc1.at[pl.ds(0, n), 0], 2 * unit1, [WINDOW[2]],
+        lambda: (c1_far(), c1_own()), lambda: go_c2(WINDOW[3]),
+    )
+    deal_s2, go_s2 = trains(
+        2, "z", "y", stage_s2, lambda r, p: ws2.at[r, p], lambda n: ws2.at[0, pl.ds(0, n)], 2 * unit1, [0],
         lambda: (state_own(), state_far()),
     )
-    c1_big = ring(
-        2, "y", lambda i, h: wc1.at[pl.ds(h * quarter, quarter), i], 8 * unit1,
-        lambda: (c1_own(), c1_far()), lambda: go_c2(),
-    )
-    c2_big = ring(
-        3, "y", lambda i, h: wc2.at[pl.ds(h * quarter, quarter), i], 4 * unit1,
+    deal_c2, go_c2 = trains(
+        3, "y", "z", stage_c2, lambda r, p: wc2.at[p, r], lambda n: wc2.at[pl.ds(0, n), 0], unit1, [0],
         lambda: (conv_own(), conv_far()),
     )
-    go_s2, go_c2 = both(s2_big), both(c2_big)
-    s1_small = deal(4, "y", stage_s1, lambda i: ws1.at[z, i], unit1, s1_big)
-    c1_small = deal(5, "z", stage_c1, lambda i: wc1.at[i, y], 2 * unit1, c1_big)
-    s2_small = deal(6, "y", stage_s2, lambda i: ws2.at[z, i], 2 * unit1, lambda: go_s2())
-    c2_small = deal(7, "z", stage_c2, lambda i: wc2.at[i, y], unit1, lambda: go_c2())
 
     def begin():
-        after("s1")
-        s1_small()
-        after("c1")
-        c1_small()
-
-    def begin_second():
-        after("s2", "c2")
-        c2_small()
-        s2_small()
+        after("s1", ws1.at[0, pl.ds(0, 3)])
+        deal_s1()
+        after("c1", wc1.at[0, pl.ds(0, 3)])
+        deal_c1()
 
     at(0.0, begin)
-    at(10.0, begin_second)
+    at(WHEN[0], lambda: (after("s2", ws2.at[0, pl.ds(0, 3)]), deal_s2()))
+    at(WHEN[1], lambda: (after("c2", wc2.at[0, pl.ds(0, 3)]), deal_c2()))
 
     step = normed.shape[3]
 
     def measure():
-        after("raw", "small")
+        for name in ("raw", *SMALL):
+            after(name)
         def body(i, carry):
             part = pl.ds(pl.multiple_of(i * 16, 16), 16)
             value = raw[part, :].astype(F32)
             mean = jnp.mean(value * value, axis=1, keepdims=True)
             scale[part, :] = jnp.broadcast_to(lax.rsqrt(mean + 1e-6), (16, 128))
             return carry
-        lax.fori_loop(0, length // 16, body, 0)
+        lax.fori_loop(0, length // 16, body, 0, unroll=2)
         normalise(t)
-        for i, axis in ((1, "y"), (2, "z")):
-            hand_over(
-                i, axis, normed.at[0, t], normed.at[i, t], normed.at[i, t], length * step * 2,
-                lambda i=i: share(
-                    i, lambda c: normed.at[i, c], length, length * step * 2,
-                    (lambda: s1_far()) if i == 1 else (lambda: c1_far()),
-                ),
+        swap(1, "y", lambda: s1_far())
+        at(WHEN[2], lambda: swap(2, "z", lambda: c1_far()))
+
+    def swap(i, axis, done):
+        for half in (0, 1):
+            number = 2 * i - 2 + half
+            relay(
+                number, number, axis, normed.at[0], normed.at[i], half, length * step * 2, done
             )
+
+    def relay(number, pair, axis, mine, theirs, half, size, done):
+        part = pl.ds(half * length // 2, length // 2)
+        hand_over(
+            pair, axis, mine.at[t, part], theirs.at[t, part], theirs.at[t, part], size / 2,
+            lambda: share(number, lambda c: theirs.at[c, part], length // 2, size / 2, done),
+        )
 
     def normalise(c):
         lanes = lanes_from(c, step)
@@ -475,12 +507,12 @@
     def feed_far():
         feed_back[...] = project_in(1, ws1).astype(BF)
         hand_over(
-            3, "y", feed_back, feed_half.at[odd["y"]], feed_half.at[1 - odd["y"]],
+            4, "y", feed_back, feed_half.at[odd["y"]], feed_half.at[1 - odd["y"]],
             length * part_width * 2, lambda: recur_ready(),
         )
 
     s1_own = when_all(1, lambda: at(clock[0], feed_own, 0.6))
-    s1_far = both(lambda: at(clock[0], feed_far, 0.6))
+    s1_far = when_all(3, lambda: at(clock[0], feed_far, 0.6))
     recur_ready = both(lambda: at(clock[0], recur, 1.4))
 
     def recur():
@@ -504,15 +536,7 @@
             summed[length - 1:length, 0:flat], summed[length - 1:length, flat:2 * flat],
         )
         finals[y, :, 0:flat], finals[y, :, flat:2 * flat] = end_r, end_i
-        spread_out(
-            scan_sems(0), "y", lambda i: finals.at[i], 8 * flat, lambda: at(clock[0], scan_row, 0.1)
-        )()
-
-    def scan_sems(number):
-        return (
-            lambda d: scan_send.at[number, d - 1],
-            lambda d: scan_recv.at[number, d - 1],
-        )
+        spread_out(0, "y", finals, 8 * flat, lambda: at(clock[0], scan_row, 0.1))
 
     def scan_row():
         span_r, span_i = power_r[length - 1:length, :], power_i[length - 1:length, :]
@@ -531,9 +555,7 @@
         rows[8:9, :], rows[9:10, :] = mine_r, mine_i
         rows[10:11, :], rows[11:12, :] = jump_r, jump_i
         totals[z, :, 0:flat], totals[z, :, flat:2 * flat] = sum_r, sum_i
-        spread_out(
-            scan_sems(1), "z", lambda i: totals.at[i], 8 * flat, lambda: at(clock[0], scan_all, 2.5)
-        )()
+        spread_out(1, "z", totals, 8 * flat, lambda: at(clock[0], scan_all, 2.5))
 
     def scan_all():
         sum_r, sum_i = rows[0:1, :], rows[1:2, :]
@@ -561,14 +583,15 @@
         answer = lax.dot_general(states[...], emit[...], NT, preferred_element_type=F32)
         answer = answer + skip_gain[...] * feed[...].astype(F32)
         act_all[0, t] = jax.nn.gelu(answer).astype(BF)
-        exchange(3, "y", act_all, lambda: state_own(), lambda: state_far())
-
-    def exchange(number, axis, blocks, own, far):
+        exchange(4, 5, "y", act_all, lambda: state_own(), lambda half: state_far())
+
+    def exchange(number, pair, axis, blocks, own, far):
         amount = length * width * 2
-        hand_over(
-            number + 1, axis, blocks.at[0, t], blocks.at[1, t], blocks.at[1, t], amount,
-            lambda: share(number + 1, lambda c: blocks.at[1, c], length, amount, far),
-        )
+        for half in (0, 1):
+            relay(
+                number + 1 + half, pair + half, axis, blocks.at[0], blocks.at[1], half, amount,
+                lambda half=half: far(half),
+            )
         share(number, lambda c: blocks.at[0, c], length, amount, own)
 
     edge = halo.shape[1]
@@ -585,12 +608,12 @@
     def gate_far():
         gated_back[...] = gate(2)
         hand_over(
-            5, "z", gated_back, gated_half.at[odd["z"]], gated_half.at[1 - odd["z"]],
+            7, "z", gated_back, gated_half.at[odd["z"]], gated_half.at[1 - odd["z"]],
             length * part_width * 2, lambda: gate_ready(),
         )
 
     c1_own = when_all(1, lambda: at(clock[0], gate_own, 0.7))
-    c1_far = both(lambda: at(clock[0], gate_far, 0.7))
+    c1_far = when_all(3, lambda: at(clock[0], gate_far, 0.7))
     gate_ready = both(lambda: at(clock[0], pass_edge, 0.1))
     last = pl.ds(length - edge, edge)
 
@@ -632,14 +655,16 @@
                     answer = answer + part
             conv_all[0, t, :, lanes] = answer.astype(BF)
         exchange(
-            6, "z", conv_all, lambda: at(clock[0], lambda: channel_norm(0), 2.5),
-            lambda: at(clock[0], lambda: channel_norm(1), 2.5),
+            7, 8, "z", conv_all, lambda: at(clock[0], lambda: channel_norm(0, 0, length), 2.4),
+            lambda half: at(
+                clock[0], lambda: channel_norm(1, half * length // 2, length // 2), 1.2
+            ),
         )
 
-    def channel_norm(which):
+    def channel_norm(which, first, tall):
         count = 2 * CHIPS * width
         def body(i, carry):
-            part = pl.ds(pl.multiple_of(i * 16, 16), 16)
+            part = pl.ds(pl.multiple_of(first + i * 16, 16), 16)
             pieces = [conv_all[which, c, part, :].astype(F32) for c in range(2 * CHIPS)]
             total = pieces[0]
             for piece in pieces[1:]:
@@ -655,7 +680,7 @@
                 value = piece * scale * chan_gain[:, lanes] + chan_shift[:, lanes]
                 conv_act[which, c, part, :] = jax.nn.silu(value).astype(BF)
             return carry
-        lax.fori_loop(0, length // 16, body, 0)
+        lax.fori_loop(0, tall // 16, body, 0, unroll=2)
         (conv_far if which else conv_own)()
 
     def project(blocks, i, weights):
@@ -679,7 +704,7 @@
     def state_out_far():
         state_back[...] = state_out(1).astype(BF)
         hand_over(
-            6, "y", state_back, state_got, state_got, length * part_columns * 2, state_returned
+            10, "y", state_back, state_got, state_got, length * part_columns * 2, state_returned
         )
 
     def state_returned():
@@ -692,16 +717,16 @@
 
     def conv_out_far():
         conv_back[...] = project(conv_act, 1, wc2).astype(BF)
-        hand_over(8, "z", conv_back, conv_got, conv_got, length * part_columns * 2, conv_returned)
+        hand_over(11, "z", conv_back, conv_got, conv_got, length * part_columns * 2, conv_returned)
 
     def conv_returned():
         conv_half[1 - odd["z"]] = conv_got[...].astype(F32)
         finish_ready()
 
     state_own = both(lambda: at(clock[0], state_out_own, 0.8))
-    state_far = both(lambda: at(clock[0], state_out_far, 0.8))
+    state_far = when_all(3, lambda: at(clock[0], state_out_far, 0.8))
     conv_own = both(lambda: at(clock[0], conv_out_own, 0.6))
-    conv_far = both(lambda: at(clock[0], conv_out_far, 0.6))
+    conv_far = when_all(3, lambda: at(clock[0], conv_out_far, 0.6))
     finish_ready = when_all(4, lambda: at(clock[0], finish, 0.5))
 
     def finish():
@@ -710,11 +735,11 @@
             result[:, lanes] = (state_half[half] + conv_half[half]).astype(BF)
         load("out", result, out)
         drain(1e9)
-        after("final", "out")
-
-    at(35.0, lambda: drain(25.0))
-    at(48.0, lambda: drain(38.0))
-    at(57.0, lambda: drain(50.0))
+        for wait in closing:
+            wait()
+        after("final")
+        after("out")
+
     run()
 
 
@@ -790,16 +815,18 @@
                     ((length, columns // 2), BF),
                 )
             ),
-            dma((40,)),
-            dma((8, len(SLOTS))),
-            dma((8, len(SLOTS))),
-            dma((2, SIDE - 1)),
-            dma((2, SIDE - 1)),
+            dma((20,)),
+            dma((4,)),
+            dma((4, 23)),
             dma((2,)),
-            dma((8, 9)),
-            dma((8, 9)),
-            dma((9,)),
-            dma((9,)),
+            dma((2,)),
+            dma((2,)),
+            dma((10,)),
+            dma((10, 5)),
+            dma((12,)),
+            dma((12,)),
+            dma((4,)),
+            dma((4, 2)),
         ],
         compiler_params=pltpu.CompilerParams(
             collective_id=0, has_side_effects=True, vmem_limit_bytes=62 * 1024 * 1024

time: 101 us -> 96.1 us (0.951)
  Pallas kernels: 96.7 us -> 92.3 us
    pallas_call x1, Pallas kernels: 96.7 us -> 92.3 us  [local(): pl.pallas_call(kernel, out_shape=(jax.ShapeDtypeStruct((length, columns),...]
where the time goes in v4:
time: 96.1 us; the launch traced here: 95.9 us
  Pallas kernels  92.3 us (96%)
  local copies, waits for them, and re-layouts  2.94 us (3%)
    pallas_call x1, Pallas kernels, local(): pl.pallas_call(kernel, out_shape=(jax.ShapeDtypeStruct((length, columns),...  92.3 us
    unnamed x2, local copies, waits for them, and re-layouts  2.94 us

profile of v4, /device:TPU:1, one launch (start us, length us, event | category | flops | bytes accessed | tf_op | source)
XLA Modules:
  0.0 95.9 jit_solution(11230199268445907357)
XLA Ops:
  0.6 92.3 %mixer.1 = (bf16[192,512]{1,0:T(8,128)(2,1)}, f32[2,16,64]{2,1,0:T(8,128)}) custom-call(bf16[192,4096]{1,0:T(8,128)(2,1)} %refs_0_.1, f32[1,4096]{1,0:T(1,128)} %bitcast.8, bf16[64,256]{1,0:T(8,128)(2,1)} %refs_2_.1, bf16[64,256]{1,0:T(8,128)(2,1)} %refs_3_.1, bf16[64,256]{1,0:T(8,128)(2,1)} %refs_4_.1, f32[31,256]{1,0:T(8,128)} %refs_5_.1, ...), custom_call_target="tpu_custom_call" | custom-call | tf_op jit(solution)/shard_map/mixer/pallas_call | solution.py:767
  93.0 1.6 %copy.23 = bf16[192,512]{1,0:T(8,128)(2,1)} copy(bf16[192,512]{1,0:T(8,128)(2,1)} %get-tuple-element.4) | data formatting | bytes 393216
  94.6 1.3 %copy.24 = f32[2,16,64]{2,1,0:T(8,128)} copy(f32[2,16,64]{2,1,0:T(8,128)} %get-tuple-element.5) | data formatting | bytes 16384

commit v5 on v4

--- a/solution.py
+++ b/solution.py
@@ -11,8 +11,8 @@
 HIGHEST = lax.Precision.HIGHEST
 MESH = pl.DeviceIdType.MESH
 SIDE = 8
-WINDOW = (2, 2, 9, 2)
-WHEN = (16.0, 14.0, 12.0)
+WINDOW = (3, 2, 3, 2)
+WHEN = (16.0, 10.0, 16.0)
 CLASSES = ((0,), (1, 7, 2, 6), (3, 5, 4))
 CHIPS = 4
 NT = (((1,), (1,)), ((), ()))
@@ -110,10 +110,10 @@
                 kept.append((time, moving))
         sent[:] = kept
 
-    def transit(link, size, count=1, rate=46.6e3):
+    def transit(link, size, count=1, rate=50e3):
         begin = max(clock[0], free.get(link, 0.0))
         free[link] = begin + size * count / rate
-        return free[link] + 0.95 + 0.75 * count
+        return free[link] + (0.8 if link == "core" else 1.9) + 0.6 * (count - (link == "core"))
 
     def when_all(number, fn):
         left = [number]
@@ -305,47 +305,40 @@
 
     other = t + 1 - 2 * core
 
-    def share(number, block, tall, size, done):
-        halves = (pl.ds(0, tall // 2), pl.ds(tall // 2, tall // 2))
-        whole = pl.ds(0, tall)
+    def share(number, block, size, done):
         near_sem = tp_recv.at[number, 0]
 
-        def copy(slot, source, part, to):
+        def copy(slot, source, to):
             return remote(
-                block(source).at[part], block(source).at[part], tp_send.at[number],
-                tp_recv.at[number, slot], device(z, y, to),
+                block(source), block(source), tp_send.at[number], tp_recv.at[number, slot],
+                device(z, y, to),
             )
-
-        def from_chip(d, which):
-            return step_to(chip, -d, CHIPS) * 2 + which
 
         def near():
             bytes_of(block(pl.ds(0, CHIPS)), near_sem)
             done()
 
         latest = [0.0]
-        all_near = when_all(5, lambda: at(latest[0], near))
-
-        def to_core(source, part, amount):
-            copy(0, source, part, other).start()
-            latest[0] = max(latest[0], transit("core", amount, 1, 300e3))
+        all_near = when_all(4, lambda: at(latest[0], near))
+
+        def to_core(source):
+            copy(0, source, other).start()
+            latest[0] = max(latest[0], transit("core", size, 1, 200e3))
             all_near()
 
         def far(d):
-            copy(d, from_chip(d, core), whole, from_chip(d, core)).wait_recv()
-            half, onward, slot, hop = (0, 1, 2, 1) if d == 1 else (1, 3, 4, -1)
-            copy(slot, from_chip(d, core), halves[half], from_chip(-onward, core)).start()
-            at(transit(("x", hop), size / 2), lambda: farther(slot, half))
-            to_core(from_chip(d, core), whole, size)
-
-        def farther(slot, half):
-            copy(slot, from_chip(2, core), halves[half], other).wait_recv()
-            to_core(from_chip(2, core), halves[half], size / 2)
-
-        for d, hop in ((1, 1), (3, -1)):
-            copy(d, t, whole, step_to(chip, d, CHIPS) * 2 + core).start()
-            at(transit(("x", hop), size), lambda d=d: far(d))
-        to_core(t, whole, size)
+            source = step_to(chip, -d, CHIPS) * 2 + core
+            copy(d, source, source).wait_recv()
+            to_core(source)
+
+        for d in (2, 1, 3):
+            copy(d, t, step_to(chip, d, CHIPS) * 2 + core).start()
+            if d == 2:
+                time = 0.6 + max(transit(("x", hop), size) for hop in (1, -1))
+            else:
+                time = transit(("x", 2 - d), size)
+            at(time, lambda d=d: far(d))
+        to_core(t)
         closing.append(lambda: bytes_of(block(pl.ds(0, 2 * CHIPS - 1)), tp_send.at[number]))
 
     unit1 = ws1.shape[2] * part_width * 2
@@ -407,7 +400,7 @@
         part = pl.ds(half * length // 2, length // 2)
         hand_over(
             pair, axis, mine.at[t, part], theirs.at[t, part], theirs.at[t, part], size / 2,
-            lambda: share(number, lambda c: theirs.at[c, part], length // 2, size / 2, done),
+            lambda: share(number, lambda c: theirs.at[c, part], size / 2, done),
         )
 
     def normalise(c):
@@ -592,7 +585,7 @@
                 number + 1 + half, pair + half, axis, blocks.at[0], blocks.at[1], half, amount,
                 lambda half=half: far(half),
             )
-        share(number, lambda c: blocks.at[0, c], length, amount, own)
+        share(number, lambda c: blocks.at[0, c], amount, own)
 
     edge = halo.shape[1]
     kernel_size = conv_taps.shape[0]
@@ -822,7 +815,7 @@
             dma((2,)),
             dma((2,)),
             dma((10,)),
-            dma((10, 5)),
+            dma((10, 4)),
             dma((12,)),
             dma((12,)),
             dma((4,)),

time: 96.1 us -> 93.4 us (0.972)
  Pallas kernels: 92.3 us -> 89.6 us
    pallas_call x1, Pallas kernels: 92.3 us -> 89.6 us  [local(): pl.pallas_call(kernel, out_shape=(jax.ShapeDtypeStruct((length, columns),...]
where the time goes in v5:
time: 93.4 us; the launch traced here: 93.1 us
  Pallas kernels  89.6 us (96%)
  local copies, waits for them, and re-layouts  2.94 us (3%)
    pallas_call x1, Pallas kernels, local(): pl.pallas_call(kernel, out_shape=(jax.ShapeDtypeStruct((length, columns),...  89.6 us
    unnamed x2, local copies, waits for them, and re-layouts  2.94 us

profile of v5, /device:TPU:1, one launch (start us, length us, event | category | flops | bytes accessed | tf_op | source)
XLA Modules:
  0.0 93.1 jit_solution(2543110168717770207)
XLA Ops:
  0.6 89.6 %mixer.1 = (bf16[192,512]{1,0:T(8,128)(2,1)}, f32[2,16,64]{2,1,0:T(8,128)}) custom-call(bf16[192,4096]{1,0:T(8,128)(2,1)} %refs_0_.1, f32[1,4096]{1,0:T(1,128)} %bitcast.8, bf16[64,256]{1,0:T(8,128)(2,1)} %refs_2_.1, bf16[64,256]{1,0:T(8,128)(2,1)} %refs_3_.1, bf16[64,256]{1,0:T(8,128)(2,1)} %refs_4_.1, f32[31,256]{1,0:T(8,128)} %refs_5_.1, ...), custom_call_target="tpu_custom_call" | custom-call | tf_op jit(solution)/shard_map/mixer/pallas_call | solution.py:760
  90.2 1.6 %copy.23 = bf16[192,512]{1,0:T(8,128)(2,1)} copy(bf16[192,512]{1,0:T(8,128)(2,1)} %get-tuple-element.4) | data formatting | bytes 393216
  91.8 1.3 %copy.24 = f32[2,16,64]{2,1,0:T(8,128)} copy(f32[2,16,64]{2,1,0:T(8,128)} %get-tuple-element.5) | data formatting | bytes 16384

commit v6 on v5

--- a/solution.py
+++ b/solution.py
@@ -11,8 +11,8 @@
 HIGHEST = lax.Precision.HIGHEST
 MESH = pl.DeviceIdType.MESH
 SIDE = 8
-WINDOW = (3, 2, 3, 2)
-WHEN = (16.0, 10.0, 16.0)
+WINDOW = (3, 3, 3, 2)
+WHEN = (16.0, 14.0, 16.0)
 CLASSES = ((0,), (1, 7, 2, 6), (3, 5, 4))
 CHIPS = 4
 NT = (((1,), (1,)), ((), ()))
@@ -113,7 +113,7 @@
     def transit(link, size, count=1, rate=50e3):
         begin = max(clock[0], free.get(link, 0.0))
         free[link] = begin + size * count / rate
-        return free[link] + (0.8 if link == "core" else 1.9) + 0.6 * (count - (link == "core"))
+        return free[link] + (0.8 if link == "core" else 2.3) + 0.6 * (count - (link == "core"))
 
     def when_all(number, fn):
         left = [number]
@@ -331,7 +331,7 @@
             copy(d, source, source).wait_recv()
             to_core(source)
 
-        for d in (2, 1, 3):
+        for d in (1, 3, 2):
             copy(d, t, step_to(chip, d, CHIPS) * 2 + core).start()
             if d == 2:
                 time = 0.6 + max(transit(("x", hop), size) for hop in (1, -1))
@@ -481,7 +481,7 @@
     at(0.5, measure, 1.0)
     at(6.0, normalise_all, 1.5)
     at(8.0, tables, 1.4)
-    at(9.0, matrices, 1.0)
+    at(9.0, matrices, 1.2)
 
     chunk = 256
 
@@ -505,8 +505,8 @@
         )
 
     s1_own = when_all(1, lambda: at(clock[0], feed_own, 0.6))
-    s1_far = when_all(3, lambda: at(clock[0], feed_far, 0.6))
-    recur_ready = both(lambda: at(clock[0], recur, 1.4))
+    s1_far = when_all(3, lambda: at(clock[0], feed_far, 0.7))
+    recur_ready = both(lambda: at(clock[0], recur, 0.8))
 
     def recur():
         feed[:, 0:part_width] = feed_half[0]
@@ -548,7 +548,7 @@
         rows[8:9, :], rows[9:10, :] = mine_r, mine_i
         rows[10:11, :], rows[11:12, :] = jump_r, jump_i
         totals[z, :, 0:flat], totals[z, :, flat:2 * flat] = sum_r, sum_i
-        spread_out(1, "z", totals, 8 * flat, lambda: at(clock[0], scan_all, 2.5))
+        spread_out(1, "z", totals, 8 * flat, lambda: at(clock[0], scan_all, 1.2))
 
     def scan_all():
         sum_r, sum_i = rows[0:1, :], rows[1:2, :]
@@ -605,8 +605,8 @@
             length * part_width * 2, lambda: gate_ready(),
         )
 
-    c1_own = when_all(1, lambda: at(clock[0], gate_own, 0.7))
-    c1_far = when_all(3, lambda: at(clock[0], gate_far, 0.7))
+    c1_own = when_all(1, lambda: at(clock[0], gate_own, 1.0))
+    c1_far = when_all(3, lambda: at(clock[0], gate_far, 1.0))
     gate_ready = both(lambda: at(clock[0], pass_edge, 0.1))
     last = pl.ds(length - edge, edge)
 
@@ -617,7 +617,7 @@
                 {"sp": following, "tp": t},
             )
         )
-        at(transit(("y", 1), edge * width * 2), convolve, 0.7)
+        at(transit(("y", 1), edge * width * 2), convolve, 1.0)
         for half in (0, 1):
             lanes = slice(half * part_width, (half + 1) * part_width)
             padded[edge:edge + length, lanes] = gated_half[half].astype(F32)
@@ -648,9 +648,9 @@
                     answer = answer + part
             conv_all[0, t, :, lanes] = answer.astype(BF)
         exchange(
-            7, 8, "z", conv_all, lambda: at(clock[0], lambda: channel_norm(0, 0, length), 2.4),
+            7, 8, "z", conv_all, lambda: at(clock[0], lambda: channel_norm(0, 0, length), 1.5),
             lambda half: at(
-                clock[0], lambda: channel_norm(1, half * length // 2, length // 2), 1.2
+                clock[0], lambda: channel_norm(1, half * length // 2, length // 2), 0.8
             ),
         )
 
@@ -716,8 +716,8 @@
         conv_half[1 - odd["z"]] = conv_got[...].astype(F32)
         finish_ready()
 
-    state_own = both(lambda: at(clock[0], state_out_own, 0.8))
-    state_far = when_all(3, lambda: at(clock[0], state_out_far, 0.8))
+    state_own = both(lambda: at(clock[0], state_out_own, 1.0))
+    state_far = when_all(3, lambda: at(clock[0], state_out_far, 1.0))
     conv_own = both(lambda: at(clock[0], conv_out_own, 0.6))
     conv_far = when_all(3, lambda: at(clock[0], conv_out_far, 0.6))
     finish_ready = when_all(4, lambda: at(clock[0], finish, 0.5))

time: 93.4 us -> 94 us (level)
  no operation moved by 1% of the time
where the time goes in v6:
time: 94 us; the launch traced here: 93.8 us
  Pallas kernels  90.3 us (96%)
  local copies, waits for them, and re-layouts  2.94 us (3%)
    pallas_call x1, Pallas kernels, local(): pl.pallas_call(kernel, out_shape=(jax.ShapeDtypeStruct((length, columns),...  90.3 us
    unnamed x2, local copies, waits for them, and re-layouts  2.94 us

profile of v6, /device:TPU:1, one launch (start us, length us, event | category | flops | bytes accessed | tf_op | source)
XLA Modules:
  0.0 93.8 jit_solution(4718366122658955989)
XLA Ops:
  0.6 90.3 %mixer.1 = (bf16[192,512]{1,0:T(8,128)(2,1)}, f32[2,16,64]{2,1,0:T(8,128)}) custom-call(bf16[192,4096]{1,0:T(8,128)(2,1)} %refs_0_.1, f32[1,4096]{1,0:T(1,128)} %bitcast.8, bf16[64,256]{1,0:T(8,128)(2,1)} %refs_2_.1, bf16[64,256]{1,0:T(8,128)(2,1)} %refs_3_.1, bf16[64,256]{1,0:T(8,128)(2,1)} %refs_4_.1, f32[31,256]{1,0:T(8,128)} %refs_5_.1, ...), custom_call_target="tpu_custom_call" | custom-call | tf_op jit(solution)/shard_map/mixer/pallas_call | solution.py:760
  90.9 1.6 %copy.23 = bf16[192,512]{1,0:T(8,128)(2,1)} copy(bf16[192,512]{1,0:T(8,128)(2,1)} %get-tuple-element.4) | data formatting | bytes 393216
  92.5 1.3 %copy.24 = f32[2,16,64]{2,1,0:T(8,128)} copy(f32[2,16,64]{2,1,0:T(8,128)} %get-tuple-element.5) | data formatting | bytes 16384

commit v7 on v6

--- a/solution.py
+++ b/solution.py
@@ -11,8 +11,8 @@
 HIGHEST = lax.Precision.HIGHEST
 MESH = pl.DeviceIdType.MESH
 SIDE = 8
-WINDOW = (3, 3, 3, 2)
-WHEN = (16.0, 14.0, 16.0)
+WINDOW = (3, 3, 3, 3)
+WHEN = (10.0, 18.0, 12.0)
 CLASSES = ((0,), (1, 7, 2, 6), (3, 5, 4))
 CHIPS = 4
 NT = (((1,), (1,)), ((), ()))
@@ -49,8 +49,8 @@
     small = refs[21:21 + len(SMALL)]
     (
         ws1, wc1, ws2, wc2, stage_s1, stage_c1, stage_s2, stage_c2, raw, scale, normed, result,
-        final_state, power_r, power_i, undo_r, undo_i, drive_r, drive_i, emit, feed, scaled, summed,
-        states, rows, finals, totals, feed_half, feed_back, gated_half, gated_back, halo, padded,
+        final_half, power_r, power_i, undo_r, undo_i, drive_r, drive_i, emit, scaled, summed,
+        states, rows, finals, totals, feed_block, gated_block, halo, padded,
         shifted, conv_all, act_all, conv_act, state_half, state_back, state_got, conv_half, conv_back,
         conv_got,
         load_sem, ring_send, ring_recv, scan_send, scan_recv, halo_sem, tp_send, tp_recv, pair_send,
@@ -62,9 +62,10 @@
     chip, core = t // 2, t % 2
     length = tokens.shape[0]
     groups, wide, size = input_real.shape
-    flat = groups * size
     width = groups * wide
     part_width = width // 2
+    groups = groups // 2
+    flat = groups * size
     columns = out.shape[1]
     part_columns = columns // 2
 
@@ -173,16 +174,17 @@
     staged("c2", "z", (conv_project,), stage_c2, wc2.at[z, y], part_columns)
 
     barrier = pltpu.get_barrier_semaphore()
-    following = lax.rem(seq + 1, SIDE * SIDE)
-    preceding = lax.rem(seq + SIDE * SIDE - 1, SIDE * SIDE)
+    at_end, at_start = y // (SIDE - 1), (SIDE - 1 - y) // (SIDE - 1)
+    following = device(step_to(z, 2 * at_end, SIDE), step_to(y, 1, SIDE), t)
+    preceding = device(step_to(z, -2 * at_start, SIDE), step_to(y, -1, SIDE), t)
     partners = []
     for d in range(1, SIDE):
         partners.append(device(z, step_to(y, d, SIDE), t))
         partners.append(device(step_to(z, d, SIDE), y, t))
     for d in range(1, 2 * CHIPS):
         partners.append(device(z, y, step_to(t, d, 2 * CHIPS)))
-    partners.append({"sp": following, "tp": t})
-    partners.append({"sp": preceding, "tp": t})
+    partners.append(following)
+    partners.append(preceding)
     for partner in partners:
         pl.semaphore_signal(barrier, inc=1, device_id=partner, device_id_type=MESH)
     pl.semaphore_wait(barrier, len(partners))
@@ -191,17 +193,18 @@
         moved = step_to(here[axis], by, SIDE)
         return device(moved, y, t) if axis == "z" else device(z, moved, t)
 
-    def spread_out(number, axis, blocks, size, done):
-        position = here[axis]
-        all_others = blocks.at[pl.ds(0, SIDE - 1)]
+    def spread_out(number, axis, blocks, size, stride, done):
+        position = here[axis] // stride
+        all_others = blocks.at[pl.ds(0, SIDE // stride - 1)]
         latest = 0.0
         for d in (4, 3, 5, 2, 6, 1, 7):
-            remote(
-                blocks.at[position], blocks.at[position], scan_send.at[number],
-                scan_recv.at[number], beside(axis, d),
-            ).start()
-            direction, count = (1, d) if d <= SIDE // 2 else (-1, SIDE - d)
-            latest = max(latest, transit((axis, direction), size, count))
+            if d % stride == 0:
+                remote(
+                    blocks.at[position], blocks.at[position], scan_send.at[number],
+                    scan_recv.at[number], beside(axis, d),
+                ).start()
+                direction, count = (1, d) if d <= SIDE // 2 else (-1, SIDE - d)
+                latest = max(latest, transit((axis, direction), size, count))
 
         def arrived():
             bytes_of(all_others, scan_recv.at[number])
@@ -431,11 +434,13 @@
 
     total_tokens = length * SIDE * SIDE
 
+    own_groups = lanes_from(odd["y"], groups)
+
     def tables():
-        rate = -as_row(decay_rate[...]) / total_tokens
-        turn = as_row(frequency[...])
-        rows[0:1, :] = as_row(initial_state[0])
-        rows[1:2, :] = as_row(initial_state[1])
+        rate = -as_row(decay_rate[own_groups, :]) / total_tokens
+        turn = as_row(frequency[own_groups, :])
+        rows[0:1, :] = as_row(initial_state[0, own_groups, :])
+        rows[1:2, :] = as_row(initial_state[1, own_groups, :])
         magnitude = jnp.exp(rate)
         step_r = magnitude * jnp.cos(turn)
         step_i = magnitude * jnp.sin(turn)
@@ -470,7 +475,7 @@
         stretch = spread().astype(BF)
         def fill(source, sign, dest, lanes):
             for g in range(groups):
-                copied = jnp.dot((sign * source[g]).astype(BF), stretch, preferred_element_type=F32)
+                copied = jnp.dot((sign * source[odd["y"] * groups + g]).astype(BF), stretch, preferred_element_type=F32)
                 kept = iota((wide, flat), 1) // size == g
                 dest[g * wide:(g + 1) * wide, lanes] = jnp.where(kept, copied, 0.0).astype(BF)
         fill(input_real, 1.0, drive_r, slice(0, flat))
@@ -494,52 +499,57 @@
         return total
 
     def feed_own():
-        feed_half[odd["y"]] = project_in(0, ws1).astype(BF)
+        feed_block[odd["y"]] = project_in(0, ws1).astype(BF)
         recur_ready()
 
     def feed_far():
-        feed_back[...] = project_in(1, ws1).astype(BF)
-        hand_over(
-            4, "y", feed_back, feed_half.at[odd["y"]], feed_half.at[1 - odd["y"]],
-            length * part_width * 2, lambda: recur_ready(),
-        )
+        feed_block[1 - odd["y"]] = project_in(1, ws1).astype(BF)
+        recur_ready()
 
     s1_own = when_all(1, lambda: at(clock[0], feed_own, 0.6))
     s1_far = when_all(3, lambda: at(clock[0], feed_far, 0.7))
     recur_ready = both(lambda: at(clock[0], recur, 0.8))
+    end = slice(length - 1, length)
 
     def recur():
-        feed[:, 0:part_width] = feed_half[0]
-        feed[:, part_width:width] = feed_half[1]
-        drive = feed[...]
+        drive = feed_block[...].reshape(2 * length, part_width)
         for j in range(flat // chunk):
             part = slice(j * chunk, (j + 1) * chunk)
             shift = slice(flat + j * chunk, flat + (j + 1) * chunk)
             push_r = jnp.dot(drive, drive_r[:, part], preferred_element_type=F32)
             push_i = jnp.dot(drive, drive_i[:, part], preferred_element_type=F32)
-            back_r, back_i = rotate(undo_r[:, part], undo_i[:, part], push_r, push_i)
-            scaled[:, part] = back_r.astype(BF)
-            scaled[:, shift] = back_i.astype(BF)
+            for b in (0, 1):
+                span = slice(b * length, (b + 1) * length)
+                back_r, back_i = rotate(
+                    undo_r[:, part], undo_i[:, part], push_r[span, :], push_i[span, :]
+                )
+                scaled[b, :, part] = back_r.astype(BF)
+                scaled[b, :, shift] = back_i.astype(BF)
         lower = (iota((length, length), 0) >= iota((length, length), 1)).astype(BF)
-        for j in range(2 * flat // chunk):
-            part = slice(j * chunk, (j + 1) * chunk)
-            summed[:, part] = jnp.dot(lower, scaled[:, part], preferred_element_type=F32)
-        end_r, end_i = rotate(
-            power_r[length - 1:length, :], power_i[length - 1:length, :],
-            summed[length - 1:length, 0:flat], summed[length - 1:length, flat:2 * flat],
-        )
-        finals[y, :, 0:flat], finals[y, :, flat:2 * flat] = end_r, end_i
-        spread_out(0, "y", finals, 8 * flat, lambda: at(clock[0], scan_row, 0.1))
+        for b in (0, 1):
+            for j in range(2 * flat // chunk):
+                part = slice(j * chunk, (j + 1) * chunk)
+                summed[b, :, part] = jnp.dot(lower, scaled[b, :, part], preferred_element_type=F32)
+        span_r, span_i = power_r[end, :], power_i[end, :]
+        first_r, first_i = rotate(span_r, span_i, summed[0, end, 0:flat], summed[0, end, flat:2 * flat])
+        second_r, second_i = rotate(span_r, span_i, summed[1, end, 0:flat], summed[1, end, flat:2 * flat])
+        rows[12:13, :], rows[13:14, :] = first_r, first_i
+        moved_r, moved_i = rotate(span_r, span_i, first_r, first_i)
+        finals[y // 2, :, 0:flat] = moved_r + second_r
+        finals[y // 2, :, flat:2 * flat] = moved_i + second_i
+        spread_out(0, "y", finals, 8 * flat, 2, lambda: at(clock[0], scan_row, 0.1))
 
     def scan_row():
-        span_r, span_i = power_r[length - 1:length, :], power_i[length - 1:length, :]
+        span_r, span_i = power_r[end, :], power_i[end, :]
+        span_r, span_i = rotate(span_r, span_i, span_r, span_i)
         zero = jnp.zeros((1, flat), F32)
         sum_r, sum_i, before_r, before_i = zero, zero, zero, zero
         jump_r, jump_i = zero + 1.0, zero
         mine_r, mine_i = zero, zero
-        for yy in range(SIDE):
-            before_r, before_i = jnp.where(y == yy, sum_r, before_r), jnp.where(y == yy, sum_i, before_i)
-            mine_r, mine_i = jnp.where(y == yy, jump_r, mine_r), jnp.where(y == yy, jump_i, mine_i)
+        for yy in range(SIDE // 2):
+            here_now = y // 2 == yy
+            before_r, before_i = jnp.where(here_now, sum_r, before_r), jnp.where(here_now, sum_i, before_i)
+            mine_r, mine_i = jnp.where(here_now, jump_r, mine_r), jnp.where(here_now, jump_i, mine_i)
             next_r, next_i = rotate(span_r, span_i, sum_r, sum_i)
             sum_r = next_r + finals[yy, :, 0:flat]
             sum_i = next_i + finals[yy, :, flat:2 * flat]
@@ -548,7 +558,7 @@
         rows[8:9, :], rows[9:10, :] = mine_r, mine_i
         rows[10:11, :], rows[11:12, :] = jump_r, jump_i
         totals[z, :, 0:flat], totals[z, :, flat:2 * flat] = sum_r, sum_i
-        spread_out(1, "z", totals, 8 * flat, lambda: at(clock[0], scan_all, 1.2))
+        spread_out(1, "z", totals, 8 * flat, 1, lambda: at(clock[0], scan_all, 1.2))
 
     def scan_all():
         sum_r, sum_i = rows[0:1, :], rows[1:2, :]
@@ -559,33 +569,63 @@
             next_r, next_i = rotate(jump_r, jump_i, sum_r, sum_i)
             sum_r = next_r + totals[zz, :, 0:flat]
             sum_i = next_i + totals[zz, :, flat:2 * flat]
-        final_state[0] = as_table(sum_r)
-        final_state[1] = as_table(sum_i)
-        load("final", final_state, final_out)
+        final_half[odd["y"], 0] = as_table(sum_r)
+        final_half[odd["y"], 1] = as_table(sum_i)
+        hand_over(
+            4, "y", final_half.at[odd["y"]], final_half.at[odd["y"]], final_half.at[1 - odd["y"]],
+            8 * flat, store_final,
+        )
         lead_r, lead_i = rotate(rows[8:9, :], rows[9:10, :], start_r, start_i)
         entry_r, entry_i = lead_r + rows[6:7, :], lead_i + rows[7:8, :]
-        for j in range(flat // chunk):
-            part = slice(j * chunk, (j + 1) * chunk)
-            shift = slice(flat + j * chunk, flat + (j + 1) * chunk)
-            state_r, state_i = rotate(
-                power_r[:, part], power_i[:, part],
-                summed[:, part] + entry_r[:, part], summed[:, shift] + entry_i[:, part],
+        next_r, next_i = rotate(power_r[end, :], power_i[end, :], entry_r, entry_i)
+        entries = ((entry_r, entry_i), (next_r + rows[12:13, :], next_i + rows[13:14, :]))
+        for b in (0, 1):
+            into_r, into_i = entries[b]
+            for j in range(flat // chunk):
+                part = slice(j * chunk, (j + 1) * chunk)
+                shift = slice(flat + j * chunk, flat + (j + 1) * chunk)
+                state_r, state_i = rotate(
+                    power_r[:, part], power_i[:, part],
+                    summed[b, :, part] + into_r[:, part], summed[b, :, shift] + into_i[:, part],
+                )
+                states[b, :, part] = state_r.astype(BF)
+                states[b, :, shift] = state_i.astype(BF)
+        answer = lax.dot_general(
+            states[...].reshape(2 * length, 2 * flat), emit[...], NT, preferred_element_type=F32
+        )
+        direct = skip_gain[:, lanes_from(odd["y"], part_width)]
+        answer = answer + direct * feed_block[...].reshape(2 * length, part_width).astype(F32)
+        act_all[odd["y"], t] = jax.nn.gelu(answer).astype(BF).reshape(2, length, part_width)
+        exchange(
+            4, 5, "y", act_all, lambda: (state_far(), state_own()),
+            lambda own: state_own() if own else state_far(),
+        )
+
+    def store_final():
+        for half in (0, 1):
+            load(
+                "final" + str(half), final_half.at[half],
+                final_out.at[:, pl.ds(half * groups, groups)],
             )
-            states[:, part] = state_r.astype(BF)
-            states[:, shift] = state_i.astype(BF)
-        answer = lax.dot_general(states[...], emit[...], NT, preferred_element_type=F32)
-        answer = answer + skip_gain[...] * feed[...].astype(F32)
-        act_all[0, t] = jax.nn.gelu(answer).astype(BF)
-        exchange(4, 5, "y", act_all, lambda: state_own(), lambda half: state_far())
-
-    def exchange(number, pair, axis, blocks, own, far):
-        amount = length * width * 2
-        for half in (0, 1):
-            relay(
-                number + 1 + half, pair + half, axis, blocks.at[0], blocks.at[1], half, amount,
-                lambda half=half: far(half),
+
+    def exchange(number, pair, axis, blocks, shared, relayed):
+        amount = 2 * length * part_width * 2
+        mine = odd[axis]
+
+        def relay_block(i):
+            sent_block, got_block = (mine, 1 - mine) if i == 0 else (1 - mine, mine)
+            hand_over(
+                pair + i, axis, blocks.at[mine, t, sent_block], blocks.at[mine, t, sent_block],
+                blocks.at[1 - mine, t, got_block], amount / 2,
+                lambda: share(
+                    number + 1 + i, lambda c: blocks.at[1 - mine, c, got_block], amount / 2,
+                    lambda: relayed(i),
+                ),
             )
-        share(number, lambda c: blocks.at[0, c], amount, own)
+
+        relay_block(0)
+        relay_block(1)
+        share(number, lambda c: blocks.at[mine, c], amount, shared)
 
     edge = halo.shape[1]
     kernel_size = conv_taps.shape[0]
@@ -595,15 +635,12 @@
         return (pair[:, 0:part_width] * jax.nn.sigmoid(pair[:, part_width:width])).astype(BF)
 
     def gate_own():
-        gated_half[odd["z"]] = gate(0)
+        gated_block[odd["z"]] = gate(0)
         gate_ready()
 
     def gate_far():
-        gated_back[...] = gate(2)
-        hand_over(
-            7, "z", gated_back, gated_half.at[odd["z"]], gated_half.at[1 - odd["z"]],
-            length * part_width * 2, lambda: gate_ready(),
-        )
+        gated_block[1 - odd["z"]] = gate(2)
+        gate_ready()
 
     c1_own = when_all(1, lambda: at(clock[0], gate_own, 1.0))
     c1_far = when_all(3, lambda: at(clock[0], gate_far, 1.0))
@@ -611,54 +648,53 @@
     last = pl.ds(length - edge, edge)
 
     def pass_edge():
-        start(
-            remote(
-                gated_half.at[:, last], halo, halo_sem.at[0], halo_sem.at[1],
-                {"sp": following, "tp": t},
+        for b, to, slot in (
+            (0, beside("y", 1), at_end),
+            (1, following, 1 - at_end),
+        ):
+            start(
+                remote(
+                    gated_block.at[b, last], halo.at[slot], halo_sem.at[b], halo_sem.at[2 + slot], to
+                )
             )
-        )
-        at(transit(("y", 1), edge * width * 2), convolve, 1.0)
-        for half in (0, 1):
-            lanes = slice(half * part_width, (half + 1) * part_width)
-            padded[edge:edge + length, lanes] = gated_half[half].astype(F32)
+        at(transit(("y", 1), 2 * edge * part_width * 2), convolve, 1.0)
+        for b in (0, 1):
+            padded[b, edge:edge + length, :] = gated_block[b].astype(F32)
 
     def convolve():
-        remote(
-            gated_half.at[:, last], halo, halo_sem.at[0], halo_sem.at[1],
-            {"sp": preceding, "tp": t},
-        ).wait_recv()
-        for half in (0, 1):
-            lanes = slice(half * part_width, (half + 1) * part_width)
-            padded[0:edge, lanes] = jnp.where(seq > 0, halo[half].astype(F32), 0.0)
+        for slot in (0, 1):
+            bytes_of(halo.at[slot], halo_sem.at[2 + slot])
+        padded[0, 0:edge, :] = jnp.where(z // 2 + y > 0, halo[0].astype(F32), 0.0)
+        padded[1, 0:edge, :] = halo[1].astype(F32)
+        taps = conv_taps[:, lanes_from(odd["z"], part_width)]
         lag = edge - (kernel_size - 1)
-        for lane in range(width // 128):
-            lanes = slice(lane * 128, (lane + 1) * 128)
-            answer = jnp.zeros((length, 128), F32)
+        for block in (0, 1):
+            answer = jnp.zeros((length, part_width), F32)
             for b in range(8):
                 tall = length + (8 if b else 0)
-                part = jnp.zeros((tall, 128), F32)
+                part = jnp.zeros((tall, part_width), F32)
                 for a in range(edge // 8 + 1):
                     k = 8 * a + b - lag
                     if 0 <= k < kernel_size:
-                        part = part + conv_taps[k:k + 1, lanes] * padded[8 * a:8 * a + tall, lanes]
+                        part = part + taps[k:k + 1, :] * padded[block, 8 * a:8 * a + tall, :]
                 if b:
                     shifted[b, :, :] = part
                     answer = answer + shifted[b, b:b + length, :]
                 else:
                     answer = answer + part
-            conv_all[0, t, :, lanes] = answer.astype(BF)
+            conv_all[odd["z"], t, block] = answer.astype(BF)
         exchange(
-            7, 8, "z", conv_all, lambda: at(clock[0], lambda: channel_norm(0, 0, length), 1.5),
-            lambda half: at(
-                clock[0], lambda: channel_norm(1, half * length // 2, length // 2), 0.8
-            ),
+            7, 8, "z", conv_all, lambda: (norm_far(), norm_own()),
+            lambda own: norm_own() if own else norm_far(),
         )
 
-    def channel_norm(which, first, tall):
+    def channel_norm(which, own):
         count = 2 * CHIPS * width
         def body(i, carry):
-            part = pl.ds(pl.multiple_of(first + i * 16, 16), 16)
-            pieces = [conv_all[which, c, part, :].astype(F32) for c in range(2 * CHIPS)]
+            part = pl.ds(pl.multiple_of(i * 16, 16), 16)
+            pieces = [
+                conv_all[c % 2, c // 2, which, part, :].astype(F32) for c in range(4 * CHIPS)
+            ]
             total = pieces[0]
             for piece in pieces[1:]:
                 total = total + piece
@@ -669,33 +705,37 @@
                 total = total + piece * piece
             scale = lax.rsqrt(jnp.sum(total, axis=1, keepdims=True) / count + 1e-5)
             for c, piece in enumerate(pieces):
-                lanes = slice(c * width, (c + 1) * width)
+                lanes = slice(c * part_width, (c + 1) * part_width)
                 value = piece * scale * chan_gain[:, lanes] + chan_shift[:, lanes]
-                conv_act[which, c, part, :] = jax.nn.silu(value).astype(BF)
+                half = slice(c % 2 * part_width, (c % 2 + 1) * part_width)
+                conv_act[which, c // 2, part, half] = jax.nn.silu(value).astype(BF)
             return carry
-        lax.fori_loop(0, tall // 16, body, 0, unroll=2)
-        (conv_far if which else conv_own)()
-
-    def project(blocks, i, weights):
+        lax.fori_loop(0, length // 16, body, 0, unroll=2)
+        (conv_own if own else conv_far)()
+
+    norm_own = both(lambda: at(clock[0], lambda: channel_norm(odd["z"], True), 1.5))
+    norm_far = both(lambda: at(clock[0], lambda: channel_norm(1 - odd["z"], False), 1.5))
+
+    def project(piece, weights):
         count = weights.shape[3]
         total = None
         for c in range(2 * CHIPS):
-            term = jnp.dot(
-                blocks[i, c], weights[c].reshape(width, count), preferred_element_type=F32
-            )
+            term = jnp.dot(piece(c), weights[c].reshape(width, count), preferred_element_type=F32)
             total = term if total is None else total + term
         return total
 
     def state_out(i):
-        pair = project(act_all, i, ws2)
+        pair = project(
+            lambda c: jnp.concatenate([act_all[0, c, i], act_all[1, c, i]], axis=1), ws2
+        )
         return pair[:, 0:part_columns] * jax.nn.sigmoid(pair[:, part_columns:columns])
 
     def state_out_own():
-        state_half[odd["y"]] = state_out(0)
+        state_half[odd["y"]] = state_out(odd["y"])
         finish_ready()
 
     def state_out_far():
-        state_back[...] = state_out(1).astype(BF)
+        state_back[...] = state_out(1 - odd["y"]).astype(BF)
         hand_over(
             10, "y", state_back, state_got, state_got, length * part_columns * 2, state_returned
         )
@@ -705,21 +745,21 @@
         finish_ready()
 
     def conv_out_own():
-        conv_half[odd["z"]] = project(conv_act, 0, wc2)
+        conv_half[odd["z"]] = project(lambda c: conv_act[odd["z"], c], wc2)
         finish_ready()
 
     def conv_out_far():
-        conv_back[...] = project(conv_act, 1, wc2).astype(BF)
+        conv_back[...] = project(lambda c: conv_act[1 - odd["z"], c], wc2).astype(BF)
         hand_over(11, "z", conv_back, conv_got, conv_got, length * part_columns * 2, conv_returned)
 
     def conv_returned():
         conv_half[1 - odd["z"]] = conv_got[...].astype(F32)
         finish_ready()
 
-    state_own = both(lambda: at(clock[0], state_out_own, 1.0))
+    state_own = when_all(3, lambda: at(clock[0], state_out_own, 1.0))
     state_far = when_all(3, lambda: at(clock[0], state_out_far, 1.0))
     conv_own = both(lambda: at(clock[0], conv_out_own, 0.6))
-    conv_far = when_all(3, lambda: at(clock[0], conv_out_far, 0.6))
+    conv_far = both(lambda: at(clock[0], conv_out_far, 0.6))
     finish_ready = when_all(4, lambda: at(clock[0], finish, 0.5))
 
     def finish():
@@ -730,7 +770,8 @@
         drain(1e9)
         for wait in closing:
             wait()
-        after("final")
+        after("final0")
+        after("final1")
         after("out")
 
     run()
@@ -743,7 +784,7 @@
 ):
     length, features = tokens.shape
     groups, size, wide = input_real.shape
-    flat, width = groups * size, groups * wide
+    flat, width = groups // 2 * size, groups * wide
     deep1, columns = conv_value.shape[0], conv_project.shape[1]
     deep2 = conv_project.shape[0]
     edge = 32
@@ -779,26 +820,25 @@
             vmem((length, 128), F32),
             vmem((3, many, length, features // many), BF),
             vmem((length, columns), BF),
-            vmem(initial_state.shape, F32),
+            vmem((2, 2, groups // 2, size), F32),
             *(vmem((length, flat), F32) for _ in range(4)),
-            vmem((width, flat), BF),
-            vmem((width, flat), BF),
-            vmem((width, 2 * flat), BF),
-            vmem((length, width), BF),
-            vmem((length, 2 * flat), BF),
-            vmem((length, 2 * flat), F32),
-            vmem((length, 2 * flat), BF),
+            vmem((width // 2, flat), BF),
+            vmem((width // 2, flat), BF),
+            vmem((width // 2, 2 * flat), BF),
+            vmem((2, length, 2 * flat), BF),
+            vmem((2, length, 2 * flat), F32),
+            vmem((2, length, 2 * flat), BF),
             vmem((16, flat), F32),
-            vmem((SIDE, 1, 2 * flat), F32),
+            vmem((SIDE // 2, 1, 2 * flat), F32),
             vmem((SIDE, 1, 2 * flat), F32),
             vmem((2, length, width // 2), BF),
-            vmem((length, width // 2), BF),
             vmem((2, length, width // 2), BF),
-            vmem((length, width // 2), BF),
             vmem((2, edge, width // 2), BF),
-            vmem((edge + length, width), F32),
-            vmem((8, length + 8, 128), F32),
-            *(vmem((2, many, length, width), BF) for _ in range(3)),
+            vmem((2, edge + length, width // 2), F32),
+            vmem((8, length + 8, width // 2), F32),
+            vmem((2, many, 2, length, width // 2), BF),
+            vmem((2, many, 2, length, width // 2), BF),
+            vmem((2, many, length, width), BF),
             *(
                 vmem(shape, held)
                 for _ in range(2)
@@ -813,7 +853,7 @@
             dma((4, 23)),
             dma((2,)),
             dma((2,)),
-            dma((2,)),
+            dma((4,)),
             dma((10,)),
             dma((10, 4)),
             dma((12,)),

time: 94 us -> 88.8 us (0.945)
  Pallas kernels: 90.3 us -> 85 us
    pallas_call x1, Pallas kernels: 90.3 us -> 85 us  [local(): pl.pallas_call(kernel, out_shape=(jax.ShapeDtypeStruct((length, columns),...]
where the time goes in v7:
time: 88.8 us; the launch traced here: 88.6 us
  Pallas kernels  85 us (96%)
  local copies, waits for them, and re-layouts  2.94 us (3%)
    pallas_call x1, Pallas kernels, local(): pl.pallas_call(kernel, out_shape=(jax.ShapeDtypeStruct((length, columns),...  85 us
    unnamed x2, local copies, waits for them, and re-layouts  2.94 us

profile of v7, /device:TPU:1, one launch (start us, length us, event | category | flops | bytes accessed | tf_op | source)
XLA Modules:
  0.0 88.6 jit_solution(8268259858581878793)
XLA Ops:
  0.6 85.0 %mixer.1 = (bf16[192,512]{1,0:T(8,128)(2,1)}, f32[2,16,64]{2,1,0:T(8,128)}) custom-call(bf16[192,4096]{1,0:T(8,128)(2,1)} %refs_0_.1, f32[1,4096]{1,0:T(1,128)} %bitcast.8, bf16[64,256]{1,0:T(8,128)(2,1)} %refs_2_.1, bf16[64,256]{1,0:T(8,128)(2,1)} %refs_3_.1, bf16[64,256]{1,0:T(8,128)(2,1)} %refs_4_.1, f32[31,256]{1,0:T(8,128)} %refs_5_.1, ...), custom_call_target="tpu_custom_call" | custom-call | tf_op jit(solution)/shard_map/mixer/pallas_call | solution.py:801
  85.6 1.6 %copy.23 = bf16[192,512]{1,0:T(8,128)(2,1)} copy(bf16[192,512]{1,0:T(8,128)(2,1)} %get-tuple-element.4) | data formatting | bytes 393216
  87.2 1.3 %copy.24 = f32[2,16,64]{2,1,0:T(8,128)} copy(f32[2,16,64]{2,1,0:T(8,128)} %get-tuple-element.5) | data formatting | bytes 16384

commit v8 on v7

--- a/solution.py
+++ b/solution.py
@@ -11,8 +11,8 @@
 HIGHEST = lax.Precision.HIGHEST
 MESH = pl.DeviceIdType.MESH
 SIDE = 8
-WINDOW = (3, 3, 3, 3)
-WHEN = (10.0, 18.0, 12.0)
+WINDOW = (3, 2, 3, 3)
+WHEN = (24.0, 30.0, 2.0)
 CLASSES = ((0,), (1, 7, 2, 6), (3, 5, 4))
 CHIPS = 4
 NT = (((1,), (1,)), ((), ()))
@@ -114,7 +114,8 @@
     def transit(link, size, count=1, rate=50e3):
         begin = max(clock[0], free.get(link, 0.0))
         free[link] = begin + size * count / rate
-        return free[link] + (0.8 if link == "core" else 2.3) + 0.6 * (count - (link == "core"))
+        fixed = 1.5 if link == "core" else 4.0 if link[0] == "x" else 2.9
+        return free[link] + fixed + 0.6 * (count - 1)
 
     def when_all(number, fn):
         left = [number]
@@ -299,7 +300,7 @@
 
     def hand_over(number, axis, src, dst, landing, size, done):
         start(remote(src, dst, pair_send.at[number], pair_recv.at[number], mate(axis)))
-        time = max(transit((axis, 1), size), transit((axis, -1), size))
+        time = 0.6 + max(transit((axis, 1), size), transit((axis, -1), size))
 
         def arrived():
             remote(src, landing, pair_send.at[number], pair_recv.at[number], mate(axis)).wait_recv()
@@ -308,7 +309,7 @@
 
     other = t + 1 - 2 * core
 
-    def share(number, block, size, done):
+    def share(number, block, size, done, later=None):
         near_sem = tp_recv.at[number, 0]
 
         def copy(slot, source, to):
@@ -318,7 +319,10 @@
             )
 
         def near():
-            bytes_of(block(pl.ds(0, CHIPS)), near_sem)
+            if later is None:
+                bytes_of(block(pl.ds(0, CHIPS)), near_sem)
+            else:
+                later.append(lambda: bytes_of(block(pl.ds(0, CHIPS)), near_sem))
             done()
 
         latest = [0.0]
@@ -392,19 +396,19 @@
         swap(1, "y", lambda: s1_far())
         at(WHEN[2], lambda: swap(2, "z", lambda: c1_far()))
 
+    owed = {"y": [], "z": []}
+
     def swap(i, axis, done):
         for half in (0, 1):
             number = 2 * i - 2 + half
-            relay(
-                number, number, axis, normed.at[0], normed.at[i], half, length * step * 2, done
+            part = pl.ds(half * length // 2, length // 2)
+            block = normed.at[i, t, part]
+            hand_over(
+                number, axis, normed.at[0, t, part], block, block, length * step,
+                lambda number=number, part=part: share(
+                    number, lambda c: normed.at[i, c, part], length * step, done, owed[axis]
+                ),
             )
-
-    def relay(number, pair, axis, mine, theirs, half, size, done):
-        part = pl.ds(half * length // 2, length // 2)
-        hand_over(
-            pair, axis, mine.at[t, part], theirs.at[t, part], theirs.at[t, part], size / 2,
-            lambda: share(number, lambda c: theirs.at[c, part], size / 2, done),
-        )
 
     def normalise(c):
         lanes = lanes_from(c, step)
@@ -503,6 +507,8 @@
         recur_ready()
 
     def feed_far():
+        for wait in owed["y"]:
+            wait()
         feed_block[1 - odd["y"]] = project_in(1, ws1).astype(BF)
         recur_ready()
 
@@ -639,6 +645,8 @@
         gate_ready()
 
     def gate_far():
+        for wait in owed["z"]:
+            wait()
         gated_block[1 - odd["z"]] = gate(2)
         gate_ready()
 
@@ -777,6 +785,11 @@
     run()
 
 
+def settle(mixed, final, out, final_out):
+    out[...] = mixed[...]
+    final_out[...] = final[...]
+
+
 def local(
     tokens, norm_gain, conv_value, conv_gate, state_feed, conv_taps, chan_gain, chan_shift,
     conv_project, decay_rate, frequency, input_real, input_imag, output_real, output_imag,
@@ -798,7 +811,7 @@
     vmem = pltpu.VMEM
     dma = pltpu.SemaphoreType.DMA
     many = 2 * CHIPS
-    return pl.pallas_call(
+    mixed, final = pl.pallas_call(
         kernel,
         out_shape=(
             jax.ShapeDtypeStruct((length, columns), BF),
@@ -866,6 +879,16 @@
         ),
         name="mixer",
     )(*args)
+    return pl.pallas_call(
+        settle,
+        out_shape=(
+            jax.ShapeDtypeStruct(mixed.shape, mixed.dtype),
+            jax.ShapeDtypeStruct(final.shape, final.dtype),
+        ),
+        in_specs=[pl.BlockSpec(memory_space=vmem)] * 2,
+        out_specs=(pl.BlockSpec(memory_space=vmem),) * 2,
+        name="settle",
+    )(mixed, final)
 
 
 def solution(mesh):

time: 88.8 us -> 85.8 us (0.966)
  local copies, waits for them, and re-layouts: 2.94 us -> 0 us
    unnamed x2 -> x0, local copies, waits for them, and re-layouts: 2.94 us -> none
    pallas_call x0 -> x1, Pallas kernels: none -> 1.62 us  [local(): pl.pallas_call(settle, out_shape=(jax.ShapeDtypeStruct(mixed.shape, mixed...]
    pallas_call x1, Pallas kernels: 85 us -> 83.4 us  [local(): pl.pallas_call(kernel, out_shape=(jax.ShapeDtypeStruct((length, columns),...]
where the time goes in v8:
time: 85.8 us; the launch traced here: 85.6 us
  Pallas kernels  85 us (99%)
    pallas_call x1, Pallas kernels, local(): pl.pallas_call(kernel, out_shape=(jax.ShapeDtypeStruct((length, columns),...  83.4 us

profile of v8, /device:TPU:1, one launch (start us, length us, event | category | flops | bytes accessed | tf_op | source)
XLA Modules:
  0.0 85.6 jit_solution(4270299148241437249)
XLA Ops:
  0.6 83.4 %mixer.1 = (bf16[192,512]{1,0:T(8,128)(2,1)}, f32[2,16,64]{2,1,0:T(8,128)}) custom-call(bf16[192,4096]{1,0:T(8,128)(2,1)} %refs_0_.1, f32[1,4096]{1,0:T(1,128)} %bitcast.8, bf16[64,256]{1,0:T(8,128)(2,1)} %refs_2_.1, bf16[64,256]{1,0:T(8,128)(2,1)} %refs_3_.1, bf16[64,256]{1,0:T(8,128)(2,1)} %refs_4_.1, f32[31,256]{1,0:T(8,128)} %refs_5_.1, ...), custom_call_target="tpu_custom_call" | custom-call | tf_op jit(solution)/shard_map/mixer/pallas_call | solution.py:814
  84.0 1.6 %settle.1 = (bf16[192,512]{1,0:T(8,128)(2,1)}, f32[2,16,64]{2,1,0:T(8,128)}) custom-call(bf16[192,512]{1,0:T(8,128)(2,1)} %get-tuple-element.4.mixed, f32[2,16,64]{2,1,0:T(8,128)} %get-tuple-element.5.final), custom_call_target="tpu_custom_call" | custom-call | tf_op jit(solution)/shard_map/settle/pallas_call | solution.py:882

commit v9 on v8

--- a/solution.py
+++ b/solution.py
@@ -188,6 +188,17 @@
     partners.append(preceding)
     for partner in partners:
         pl.semaphore_signal(barrier, inc=1, device_id=partner, device_id_type=MESH)
+    def row_scales():
+        after("raw")
+        def body(i, carry):
+            part = pl.ds(pl.multiple_of(i * 16, 16), 16)
+            value = raw[part, :].astype(F32)
+            mean = jnp.mean(value * value, axis=1, keepdims=True)
+            scale[part, :] = jnp.broadcast_to(lax.rsqrt(mean + 1e-6), (16, 128))
+            return carry
+        lax.fori_loop(0, length // 16, body, 0, unroll=2)
+
+    row_scales()
     pl.semaphore_wait(barrier, len(partners))
 
     def beside(axis, by):
@@ -383,15 +394,8 @@
     step = normed.shape[3]
 
     def measure():
-        for name in ("raw", *SMALL):
+        for name in SMALL:
             after(name)
-        def body(i, carry):
-            part = pl.ds(pl.multiple_of(i * 16, 16), 16)
-            value = raw[part, :].astype(F32)
-            mean = jnp.mean(value * value, axis=1, keepdims=True)
-            scale[part, :] = jnp.broadcast_to(lax.rsqrt(mean + 1e-6), (16, 128))
-            return carry
-        lax.fori_loop(0, length // 16, body, 0, unroll=2)
         normalise(t)
         swap(1, "y", lambda: s1_far())
         at(WHEN[2], lambda: swap(2, "z", lambda: c1_far()))
@@ -487,7 +491,7 @@
         fill(output_real, 1.0, emit, slice(0, flat))
         fill(output_imag, -1.0, emit, slice(flat, 2 * flat))
 
-    at(0.5, measure, 1.0)
+    at(0.3, measure, 0.2)
     at(6.0, normalise_all, 1.5)
     at(8.0, tables, 1.4)
     at(9.0, matrices, 1.2)
@@ -718,7 +722,7 @@
                 half = slice(c % 2 * part_width, (c % 2 + 1) * part_width)
                 conv_act[which, c // 2, part, half] = jax.nn.silu(value).astype(BF)
             return carry
-        lax.fori_loop(0, length // 16, body, 0, unroll=2)
+        lax.fori_loop(0, length // 16, body, 0, unroll=4)
         (conv_own if own else conv_far)()
 
     norm_own = both(lambda: at(clock[0], lambda: channel_norm(odd["z"], True), 1.5))

time: 85.8 us -> 85.4 us (level)
  no operation moved by 1% of the time
where the time goes in v9:
time: 85.4 us; the launch traced here: 85.1 us
  Pallas kernels  84.5 us (99%)
    pallas_call x1, Pallas kernels, local(): pl.pallas_call(kernel, out_shape=(jax.ShapeDtypeStruct((length, columns),...  82.9 us

profile of v9, /device:TPU:1, one launch (start us, length us, event | category | flops | bytes accessed | tf_op | source)
XLA Modules:
  0.0 85.1 jit_solution(1549144865600332704)
XLA Ops:
  0.6 82.9 %mixer.1 = (bf16[192,512]{1,0:T(8,128)(2,1)}, f32[2,16,64]{2,1,0:T(8,128)}) custom-call(bf16[192,4096]{1,0:T(8,128)(2,1)} %refs_0_.1, f32[1,4096]{1,0:T(1,128)} %bitcast.8, bf16[64,256]{1,0:T(8,128)(2,1)} %refs_2_.1, bf16[64,256]{1,0:T(8,128)(2,1)} %refs_3_.1, bf16[64,256]{1,0:T(8,128)(2,1)} %refs_4_.1, f32[31,256]{1,0:T(8,128)} %refs_5_.1, ...), custom_call_target="tpu_custom_call" | custom-call | tf_op jit(solution)/shard_map/mixer/pallas_call | solution.py:818
  83.5 1.6 %settle.1 = (bf16[192,512]{1,0:T(8,128)(2,1)}, f32[2,16,64]{2,1,0:T(8,128)}) custom-call(bf16[192,512]{1,0:T(8,128)(2,1)} %get-tuple-element.4.mixed, f32[2,16,64]{2,1,0:T(8,128)} %get-tuple-element.5.final), custom_call_target="tpu_custom_call" | custom-call | tf_op jit(solution)/shard_map/settle/pallas_call | solution.py:886
